TPU v7x, 32 devices: a whole 2x2x4 slice. The times are simulated.
32 devices in a mesh: sp: 8 (over z, core), tp: 4 (over y, x).
Axes of the slice: x: 2, y: 2, z: 4, core: 2. Of those that a mesh axis runs over, the one named last changes fastest.
Arguments:
- b_gate: bfloat16 [2048, 1024], P('sp', 'tp'), may hold values from -6 to 6
- c_gate: bfloat16 [2048, 1024], P('sp', 'tp'), may hold values from -6 to 6
- h_in: bfloat16 [2048, 1024], P('sp', 'tp'), may hold values from -6 to 6
- docs: int32 [2048], replicated, may hold values from 0 to 3, never falling along the last dimension, each value on 1 to 1024 neighbouring positions
- conv_taps: bfloat16 [3, 1024], replicated, may hold values from -3 to 3
- out_weight: bfloat16 [1024, 4096], P(None, 'tp'), may hold values from -0.1875 to 0.1875
- residual_in: bfloat16 [2048, 4096], P('sp', 'tp'), may hold values from -52 to 52
- norm_gain: bfloat16 [4096], replicated, may hold values from 0.099609375 to 1.8984375
- expert_pick: int32 [2048, 2], P('sp'), may hold values from 0 to 7, as said below
- route_weight: float32 [2048, 2], P('sp'), may hold values from 0.5 to 2
- w_gate: bfloat16 [8, 4096, 2048], P('sp', None, 'tp'), may hold values from -0.09375 to 0.09375
- w_up: bfloat16 [8, 4096, 2048], P('sp', None, 'tp'), may hold values from -0.09375 to 0.09375
- w_down: bfloat16 [8, 2048, 4096], P('sp', None, 'tp'), may hold values from -0.125 to 0.125
Outputs:
- stream_out: bfloat16 [2048, 4096], P('sp', 'tp')
Inputs may be any that keep to these rules, and one draw needn't show every extreme that they name: `expert_pick`: each row names 2 different experts of one group; group g holds experts g * 2 up to the next group's first.
All inputs are finite; a program needn't handle non-finite values.
Results may differ from a plain program's by a relative error of at most 0.012.
Values may be sent and summed in bfloat16 or wider, within the bound.
A program may use at most 64 MiB of HBM per device.

v0:
```python
import functools

import jax
import jax.numpy as jnp
from jax import lax
from jax.experimental import pallas as pl
from jax.experimental.pallas import tpu as pltpu
from jax.sharding import PartitionSpec as P

TOP_K = 2
GROUPS = 4
MESH = pl.DeviceIdType.MESH


NORM_EPS = 1e-06


def passed_along(value, axis, steps):
    count = lax.axis_size(axis)
    first, last = (max(0, -steps), min(count, count - steps))
    return lax.ppermute(value, axis, [(source, source + steps) for source in range(first, last)])


def general(
    b_gate,
    c_gate,
    h_in,
    docs,
    conv_taps,
    out_weight,
    residual_in,
    norm_gain,
    expert_pick,
    route_weight,
    w_gate,
    w_up,
    w_down,
):
    tok_rows, local_chans = h_in.shape
    width = residual_in.shape[1]
    full_dim = w_gate.shape[1]
    n_sp = lax.axis_size("sp")
    sp_index = lax.axis_index("sp")
    tp_index = lax.axis_index("tp")
    first_pos = sp_index * tok_rows
    product = (c_gate.astype(jnp.float32) * h_in.astype(jnp.float32)).astype(jnp.bfloat16)
    edge = passed_along(product[tok_rows - 2 :], "sp", 1)
    extended = jnp.concatenate([edge, product], axis=0).astype(jnp.float32)
    own_docs = lax.dynamic_slice_in_dim(docs, first_pos, tok_rows)
    padded_docs = jnp.concatenate([jnp.full((2,), -1, jnp.int32), docs], axis=0)
    near_docs = lax.dynamic_slice_in_dim(padded_docs, first_pos, tok_rows + 2)
    tap_weights = lax.dynamic_slice_in_dim(
        conv_taps, tp_index * local_chans, local_chans, 1
    ).astype(jnp.float32)
    conv_sum = tap_weights[0][None, :] * extended[2:]
    for step_back in (1, 2):
        same_doc = (near_docs[2 - step_back : 2 - step_back + tok_rows] == own_docs).astype(
            jnp.float32
        )[:, None]
        conv_sum = (
            conv_sum
            + tap_weights[step_back][None, :]
            * extended[2 - step_back : 2 - step_back + tok_rows]
            * same_doc
        )
    conv_out = (b_gate.astype(jnp.float32) * conv_sum).astype(jnp.bfloat16)
    projected = jnp.dot(
        lax.all_gather(conv_out, "tp", axis=1, tiled=True),
        out_weight,
        preferred_element_type=jnp.float32,
    )
    stream = (residual_in.astype(jnp.float32) + projected).astype(jnp.bfloat16)
    stream_f = stream.astype(jnp.float32)
    capacity = 5 * tok_rows // (2 * n_sp)
    assign_flat = expert_pick.reshape(-1)
    onehot = (assign_flat[:, None] == jnp.arange(n_sp, dtype=jnp.int32)[None, :]).astype(jnp.int32)
    slot_pos = jnp.sum((jnp.cumsum(onehot, axis=0) - onehot) * onehot, axis=1)
    kept_mask = slot_pos < capacity
    target = jnp.where(
        kept_mask, assign_flat * capacity + jnp.minimum(slot_pos, capacity - 1), n_sp * capacity
    )
    table = (
        jnp.full((n_sp * capacity + 1,), -1, jnp.int32)
        .at[target]
        .set(jnp.arange(assign_flat.shape[0], dtype=jnp.int32))[:-1]
    )
    filled = table >= 0
    source_rows = jnp.maximum(table, 0) // TOP_K
    gate_local = w_gate[0]
    up_local = w_up[0]
    slot_rows = n_sp * capacity
    squares = lax.psum(jnp.sum(stream_f * stream_f, axis=1), "tp")
    inverse = lax.rsqrt(squares / full_dim + NORM_EPS)[:, None]
    gain_cols = lax.dynamic_slice_in_dim(norm_gain, tp_index * width, width).astype(jnp.float32)
    normed = (stream_f * inverse * gain_cols[None, :]).astype(jnp.bfloat16)
    outgoing = jnp.where(filled[:, None], normed[source_rows], jnp.zeros((), normed.dtype)).reshape(
        n_sp, capacity, width
    )
    received = lax.all_to_all(outgoing, "sp", split_axis=0, concat_axis=0, tiled=True)
    shard_piece = lax.all_gather(received, "tp", axis=2, tiled=True)
    flat_piece = shard_piece.reshape(slot_rows, shard_piece.shape[2])
    gate_pre = jnp.dot(flat_piece, gate_local, preferred_element_type=jnp.float32)
    up_pre = jnp.dot(flat_piece, up_local, preferred_element_type=jnp.float32)
    hidden = (jax.nn.silu(gate_pre) * up_pre).astype(jnp.bfloat16)
    down_local = w_down[0]
    result = jnp.dot(
        lax.all_gather(hidden, "tp", axis=1, tiled=True),
        down_local,
        preferred_element_type=jnp.float32,
    ).astype(jnp.bfloat16)
    returned = lax.all_to_all(
        result.reshape(n_sp, capacity, width), "sp", split_axis=0, concat_axis=0, tiled=True
    ).reshape(n_sp * capacity, width)
    picked = jnp.where(
        kept_mask[:, None],
        returned[jnp.minimum(target, n_sp * capacity - 1)].astype(jnp.float32),
        0.0,
    )
    weighted = picked * route_weight.reshape(-1)[:, None]
    feed_out = jnp.sum(weighted.reshape(tok_rows, TOP_K, width), axis=1)
    return (stream_f + feed_out).astype(jnp.bfloat16)


def flipped(index, mask):
    bit = 1
    while bit <= mask:
        if mask & bit:
            index = index + bit * (1 - 2 * ((index // bit) % 2))
        bit *= 2
    return index


def fused_kernel(
    n_chips,
    capacity,
    b_ref,
    c_ref,
    h_ref,
    cols_ref,
    taps_ref,
    resid_ref,
    gain_ref,
    ow_hbm,
    wg_hbm,
    wu_hbm,
    wd_hbm,
    out_ref,
    ow,
    wg,
    wu,
    wd,
    ext,
    cv,
    stream,
    acc,
    pt,
    rows_out,
    wts_out,
    rows,
    wts,
    normed,
    hid,
    e_own,
    e_send,
    e_recv,
    feed_out,
    back,
    local_sems,
    send_sems,
    recv_sems,
):
    tok_rows, chans = h_ref.shape
    width = resid_ref.shape[1]
    full = gain_ref.shape[1]
    hid_cols = wg.shape[1]
    sp = lax.axis_index("sp")
    tp = lax.axis_index("tp")
    chip = sp // 2
    core = sp % 2
    tp_x = (tp // 2) * 2 + (1 - tp % 2)
    tp_y = (1 - tp // 2) * 2 + tp % 2
    tp_d = (1 - tp // 2) * 2 + (1 - tp % 2)
    dev_x = (sp, tp_x)
    dev_y = (sp, tp_y)
    dev_s = (chip * 2 + (1 - core), tp)
    ks = list(range(n_chips))
    dev_z = [(flipped(chip, k) * 2 + core, tp) for k in ks]

    loads = []
    for i, (s, d) in enumerate(((ow_hbm, ow), (wg_hbm.at[0], wg), (wu_hbm.at[0], wu), (wd_hbm.at[0], wd))):
        cp = pltpu.make_async_copy(s, d, local_sems.at[i])
        cp.start()
        loads.append(cp)

    count = [0]
    sent = []

    def remote(s, d, dev):
        i = count[0]
        count[0] += 1
        return pltpu.make_async_remote_copy(
            src_ref=s, dst_ref=d, send_sem=send_sems.at[i], recv_sem=recv_sems.at[i],
            device_id=dev, device_id_type=MESH,
        )

    def go(s, d, dev):
        cp = remote(s, d, dev)
        cp.start()
        sent.append(cp)
        return cp

    def cols(index, size):
        return pl.ds(pl.multiple_of(index * size, 128), size)

    barrier = pltpu.get_barrier_semaphore()
    peers = [dev_x, dev_y, dev_s] + dev_z[1:]
    for dev in peers:
        pl.semaphore_signal(barrier, inc=1, device_id=dev, device_id_type=MESH)
    other = jnp.where(core == 0, sp - 1, sp + 1)
    has_other = jnp.where(core == 0, chip > 0, chip < n_chips - 1)

    @pl.when(has_other)
    def _():
        pl.semaphore_signal(barrier, inc=1, device_id=(other, tp), device_id_type=MESH)

    product = (c_ref[...].astype(jnp.float32) * h_ref[...].astype(jnp.float32)).astype(jnp.bfloat16)
    ext[8:, :] = product.astype(jnp.float32)
    pl.semaphore_wait(barrier, len(peers) + has_other.astype(jnp.int32))

    edge = remote(ext.at[pl.ds(tok_rows, 8)], ext.at[pl.ds(0, 8)], (sp + 1, tp))

    @pl.when(sp < 2 * n_chips - 1)
    def _():
        edge.start()

    lane = lax.broadcasted_iota(jnp.int32, (tok_rows, 128), 1)
    lane_f = lane.astype(jnp.float32)
    group = cols_ref[:, 2:3]
    onehot = (group == lane_f).astype(jnp.float32)
    earlier = (
        lax.broadcasted_iota(jnp.int32, (tok_rows, tok_rows), 1)
        < lax.broadcasted_iota(jnp.int32, (tok_rows, tok_rows), 0)
    ).astype(jnp.float32).astype(jnp.bfloat16)
    before = jnp.dot(earlier, onehot.astype(jnp.bfloat16), preferred_element_type=jnp.float32)
    slot = jnp.sum(before * onehot, axis=1, keepdims=True)
    for k in ks:
        here = flipped(chip, k).astype(jnp.float32)
        hit = jnp.where((group == here) & (slot == lane_f) & (lane < capacity), 1.0, 0.0)
        pt[k] = hit.astype(jnp.bfloat16)
    parts = jnp.zeros((tok_rows, 128), jnp.float32)
    for j in range(2):
        w = cols_ref[:, 3 + j : 4 + j]
        for i in range(3):
            piece = w.astype(jnp.bfloat16).astype(jnp.float32)
            parts = jnp.where(lane == 3 * j + i, piece, parts)
            w = w - piece
    parts = parts.astype(jnp.bfloat16)
    for k in ks:
        got = lax.dot_general(
            pt[k], parts, (((0,), (0,)), ((), ())), preferred_element_type=jnp.float32
        )
        wts_out[k] = got[:capacity].astype(jnp.bfloat16)
    wts[0] = wts_out[0]

    @pl.when(sp > 0)
    def _():
        edge.wait_recv()

    @pl.when(sp == 0)
    def _():
        ext[0:8, :] = jnp.zeros((8, chans), jnp.float32)

    taps = taps_ref[:, cols(tp, chans)].astype(jnp.float32)
    conv = taps[0:1, :] * ext[8 : 8 + tok_rows, :]
    for lag in (1, 2):
        conv = conv + taps[lag : lag + 1, :] * ext[8 - lag : 8 - lag + tok_rows, :] * cols_ref[:, lag - 1 : lag]
    conv = (b_ref[...].astype(jnp.float32) * conv).astype(jnp.bfloat16)
    cv[:, cols(tp, chans)] = conv

    def spread(buf, size, own_sends):
        mine = buf.at[:, cols(tp, size)]
        own_sends.append(go(mine, mine, dev_x))
        own_sends.append(go(mine, mine, dev_y))

    def relay(buf, size, sends):
        half = size // 2
        sends[1].wait_recv()
        part = buf.at[:, cols(tp_y * 2, half)]
        sends.append(go(part, part, dev_x))
        sends[0].wait_recv()
        part = buf.at[:, cols(tp_x * 2 + 1, half)]
        sends.append(go(part, part, dev_y))

    conv_sends = []
    spread(cv, chans, conv_sends)

    def proj(index):
        rows_ = pl.ds(pl.multiple_of(index * chans, 128), chans)
        return jnp.dot(cv[:, cols(index, chans)], ow[rows_, :], preferred_element_type=jnp.float32)

    loads[0].wait()
    acc[...] = resid_ref[...].astype(jnp.float32) + proj(tp)
    relay(cv, chans, conv_sends)
    acc[...] += proj(tp_x)
    acc[...] += proj(tp_y)
    conv_sends[2].wait_recv()
    conv_sends[3].wait_recv()
    stream[...] = (acc[...] + proj(tp_d)).astype(jnp.bfloat16)

    z_rows, z_wts = [None] * n_chips, [None] * n_chips
    mine = cols(tp, width)
    for k in [0] + ks[1:]:
        got = lax.dot_general(
            pt[k], stream[...], (((0,), (0,)), ((), ())), preferred_element_type=jnp.float32
        )[:capacity].astype(jnp.bfloat16)
        if k == 0:
            rows[0, 0, :, mine] = got
        else:
            rows_out[k] = got
            z_rows[k] = go(rows_out.at[k], rows.at[k, 0, :, mine], dev_z[k])
        if k == 0:
            row_sends = [[] for _ in ks]
            sis = [[] for _ in ks]
            first = True
            spread(rows.at[0, 0], width, row_sends[0])
            sis[0].append(go(rows.at[0, 0, :, mine], rows.at[0, 1, :, mine], dev_s))
    for k in ks[1:]:
        z_wts[k] = go(wts_out.at[k], wts.at[k], dev_z[k])

    def share(k, index, size):
        at = cols(index, size)
        sis[k].append(go(rows.at[k, 0, :, at], rows.at[k, 1, :, at], dev_s))

    def stage(k):
        if k > 0:
            z_rows[k].wait_recv()
            spread(rows.at[k, 0], width, row_sends[k])
            share(k, tp, width)

    def forward(k):
        relay(rows.at[k, 0], width, row_sends[k])
        share(k, tp_x, width)
        share(k, tp_y, width)

    def finish(k):
        row_sends[k][2].wait_recv()
        share(k, tp_d * 2, width // 2)
        row_sends[k][3].wait_recv()
        share(k, tp_d * 2 + 1, width // 2)

    hid_sends = [[] for _ in ks]

    def expand(k):
        for cp in sis[k]:
            cp.wait_recv()
        for p in range(2):
            def norm(r, carry, p=p):
                at = pl.ds(pl.multiple_of(r * 16, 16), 16)
                x = rows[k, p, at, :].astype(jnp.float32)
                ms = jnp.sum(x * x, axis=1, keepdims=True) / full
                inv = lax.rsqrt(ms + NORM_EPS)
                y = (x * inv * gain_ref[...]).astype(jnp.bfloat16)
                normed[pl.ds(pl.multiple_of(p * capacity + r * 16, 16), 16), :] = y
                return carry
            lax.fori_loop(0, capacity // 16, norm, 0)
        if k == 0:
            loads[1].wait()
            loads[2].wait()

        def tile(n, carry):
            at = pl.ds(pl.multiple_of(n * 256, 256), 256)
            x = normed[...]
            g = jnp.dot(x, wg[:, at], preferred_element_type=jnp.float32)
            u = jnp.dot(x, wu[:, at], preferred_element_type=jnp.float32)
            h = (g / (1.0 + jnp.exp(-g)) * u).astype(jnp.bfloat16)
            hid[k, :, pl.ds(pl.multiple_of(tp * hid_cols + n * 256, 256), 256)] = h
            return carry

        lax.fori_loop(0, hid_cols // 256, tile, 0)
        spread(hid.at[k], hid_cols, hid_sends[k])

    def hid_forward(k):
        relay(hid.at[k], hid_cols, hid_sends[k])

    e_sends = [None] * n_chips
    z_back = [None] * n_chips

    def down(k):
        hid_sends[k][2].wait_recv()
        hid_sends[k][3].wait_recv()
        if k == 0:
            loads[3].wait()

        def tile(n, carry):
            at = pl.ds(pl.multiple_of(n * 256, 256), 256)
            e = jnp.dot(hid[k], wd[:, at], preferred_element_type=jnp.float32).astype(jnp.bfloat16)
            e_own[k, :, at] = e[:capacity]
            e_send[k, :, at] = e[capacity:]
            return carry

        lax.fori_loop(0, width // 256, tile, 0)
        e_sends[k] = go(e_send.at[k], e_recv.at[k], dev_s)

    def combine(k):
        if k > 0:
            z_wts[k].wait_recv()
        w = wts[k].astype(jnp.float32)
        w_lane = lax.broadcasted_iota(jnp.int32, w.shape, 1)
        w_even = jnp.sum(jnp.where(w_lane < 3, w, 0.0), axis=1, keepdims=True)
        w_odd = jnp.sum(jnp.where((w_lane >= 3) & (w_lane < 6), w, 0.0), axis=1, keepdims=True)
        pick = core.astype(jnp.float32)
        w_mine = w_even * (1.0 - pick) + w_odd * pick
        w_other = w_odd * (1.0 - pick) + w_even * pick
        e_sends[k].wait_recv()
        f = (e_own[k].astype(jnp.float32) * w_mine + e_recv[k].astype(jnp.float32) * w_other).astype(jnp.bfloat16)
        if k == 0:
            back[0, 0:capacity, :] = f
        else:
            feed_out[k] = f
            z_back[k] = go(feed_out.at[k], back.at[k, pl.ds(0, capacity), :], dev_z[k])

    for k in ks:
        back[k, capacity:, :] = jnp.zeros((128 - capacity, width), jnp.bfloat16)

    last = n_chips - 1
    plan = sorted(
        [(3 * k, 0, stage, k) for k in ks]
        + [(3 * k + 4, 1, forward, k) for k in ks]
        + [(3 * k + 7, 2, finish, k) for k in ks]
        + [(3 * k + 9, 3, expand, k) for k in ks]
        + [(3 * k + 13, 4, hid_forward, k) for k in ks]
        + [(3 * k + 16, 5, down, k) for k in ks]
        + [(3 * k + 18, 6, combine, k) for k in ks],
        key=lambda item: item[:2],
    )
    for _, _, step, k in plan:
        step(k)

    acc[...] = stream[...].astype(jnp.float32)
    for k in ks:
        if k > 0:
            z_back[k].wait_recv()
        acc[...] += jnp.dot(pt[k], back[k], preferred_element_type=jnp.float32)
    out_ref[...] = acc[...].astype(jnp.bfloat16)

    for cp in sent:
        cp.wait_send()

    @pl.when(sp < 2 * n_chips - 1)
    def _():
        edge.wait_send()


def fused(
    b_gate,
    c_gate,
    h_in,
    docs,
    conv_taps,
    out_weight,
    residual_in,
    norm_gain,
    expert_pick,
    route_weight,
    w_gate,
    w_up,
    w_down,
):
    tok_rows, chans = h_in.shape
    width = residual_in.shape[1]
    full = w_gate.shape[1]
    hid_cols = w_gate.shape[2]
    hid_full = w_down.shape[1]
    n_sp = lax.axis_size("sp")
    n_chips = n_sp // 2
    capacity = 5 * tok_rows // (2 * n_sp)
    first_pos = lax.axis_index("sp") * tok_rows
    padded_docs = jnp.concatenate([jnp.full((2,), -1, jnp.int32), docs], axis=0)
    near = lax.dynamic_slice_in_dim(padded_docs, first_pos, tok_rows + 2)
    own = near[2:]
    even = expert_pick[:, 0] % 2 == 0
    side = jnp.stack(
        [
            (near[1:-1] == own).astype(jnp.float32),
            (near[:-2] == own).astype(jnp.float32),
            (expert_pick[:, 0] // 2).astype(jnp.float32),
            jnp.where(even, route_weight[:, 0], route_weight[:, 1]),
            jnp.where(even, route_weight[:, 1], route_weight[:, 0]),
        ],
        axis=1,
    )
    gain = norm_gain.astype(jnp.float32)[None, :]
    n_copies = 5 + 2 * (n_chips - 1) + 14 * n_chips + n_chips - 1
    vmem = pl.BlockSpec(memory_space=pltpu.VMEM)
    hbm = pl.BlockSpec(memory_space=pl.ANY)
    bf16 = jnp.bfloat16
    return pl.pallas_call(
        functools.partial(fused_kernel, n_chips, capacity),
        out_shape=jax.ShapeDtypeStruct((tok_rows, width), bf16),
        in_specs=[vmem] * 7 + [hbm] * 4,
        out_specs=vmem,
        scratch_shapes=[
            pltpu.VMEM(out_weight.shape, bf16),
            pltpu.VMEM(w_gate.shape[1:], bf16),
            pltpu.VMEM(w_up.shape[1:], bf16),
            pltpu.VMEM(w_down.shape[1:], bf16),
            pltpu.VMEM((tok_rows + 8, chans), jnp.float32),
            pltpu.VMEM((tok_rows, out_weight.shape[0]), bf16),
            pltpu.VMEM((tok_rows, width), bf16),
            pltpu.VMEM((tok_rows, width), jnp.float32),
            pltpu.VMEM((n_chips, tok_rows, 128), bf16),
            pltpu.VMEM((n_chips, capacity, width), bf16),
            pltpu.VMEM((n_chips, capacity, 128), bf16),
            pltpu.VMEM((n_chips, 2, capacity, full), bf16),
            pltpu.VMEM((n_chips, capacity, 128), bf16),
            pltpu.VMEM((2 * capacity, full), bf16),
            pltpu.VMEM((n_chips, 2 * capacity, hid_full), bf16),
            pltpu.VMEM((n_chips, capacity, width), bf16),
            pltpu.VMEM((n_chips, capacity, width), bf16),
            pltpu.VMEM((n_chips, capacity, width), bf16),
            pltpu.VMEM((n_chips, capacity, width), bf16),
            pltpu.VMEM((n_chips, 128, width), bf16),
            pltpu.SemaphoreType.DMA((4,)),
            pltpu.SemaphoreType.DMA((n_copies,)),
            pltpu.SemaphoreType.DMA((n_copies,)),
        ],
        compiler_params=pltpu.CompilerParams(
            collective_id=0, has_side_effects=True, vmem_limit_bytes=56 * 1024 * 1024
        ),
    )(b_gate, c_gate, h_in, side, conv_taps, residual_in, gain, out_weight, w_gate, w_up, w_down)


def pairs_fit(mesh):
    n_sp, n_tp = mesh.shape["sp"], mesh.shape["tp"]
    return n_sp == GROUPS * TOP_K and TOP_K == 2 and n_tp == 4


def solution(mesh):
    return jax.shard_map(
        fused if pairs_fit(mesh) else general,
        mesh=mesh,
        in_specs=(
            P("sp", "tp"),
            P("sp", "tp"),
            P("sp", "tp"),
            P(),
            P(),
            P(None, "tp"),
            P("sp", "tp"),
            P(),
            P("sp", None),
            P("sp", None),
            P("sp", None, "tp"),
            P("sp", None, "tp"),
            P("sp", None, "tp"),
        ),
        out_specs=P("sp", "tp"),
        check_vma=False,
    )
```

profile of v0, /device:TPU:0, one launch (start us, length us, event | category | flops | bytes accessed | tf_op | source)
XLA Modules:
  0.0 87.0 jit_solution(3955387450302778442)
XLA Ops:
  0.0 0.8 pad_dynamic-slice_fusion
  0.8 0.1 compare_convert_fusion
  0.8 0.8 compare_select_fusion.3
  1.6 0.8 compare_select_fusion.4
  2.4 0.7 fusion
  3.1 1.3 %broadcast_in_dim.7 = f32[4096]{0:T(1024)} convert(bf16[4096]{0:T(1024)(128)(2,1)} %param.20) | non-fusion elementwise | flops 4096 | bytes 24576 | tf_op jit(solution)/shard_map/broadcast_in_dim | solution.py:492
  4.4 0.8 copy.26.cols_ref
  5.2 80.0 %shard_map.127 = bf16[256,1024]{1,0:T(8,128)(2,1)} custom-call(bf16[256,256]{1,0:T(8,128)(2,1)} %b_ref.1, bf16[256,256]{1,0:T(8,128)(2,1)} %c_ref.1, bf16[256,256]{1,0:T(8,128)(2,1)} %h_ref.1, f32[256,5]{1,0:T(8,128)} %copy.26.cols_ref, bf16[3,1024]{1,0:T(4,128)(2,1)} %taps_ref.1, bf16[256,1024]{1,0:T(8,128)(2,1)} %resid_ref.1, f32[1,4096]{1,0:T(1,128)} %bitcast.3, ...), custom_call_target="tpu_custom_call" | custom-call | tf_op jit(solution)/shard_map/pallas_call | solution.py:497
  85.2 1.9 %copy.28 = bf16[256,1024]{1,0:T(8,128)(2,1)} copy(bf16[256,1024]{1,0:T(8,128)(2,1)} %shard_map.127) | data formatting | bytes 1048576
  (1 shorter events, 0.0 us)
where the time goes:
time: 87.9 us; the launch traced here: 87 us
  Pallas kernels  80 us (91%)
  other arithmetic  3.6 us (4%)
  local copies, waits for them, and re-layouts  3.46 us (4%)
    pallas_call x1, Pallas kernels, fused(): pl.pallas_call(functools.partial(fused_kernel, n_chips, capacity), out_sh...  80 us
    unnamed x1, local copies, waits for them, and re-layouts  1.87 us

commit v1 on v0

v1 whole, which is shorter than its diff:
```python
import functools

import jax
import jax.numpy as jnp
from jax import lax
from jax.experimental import pallas as pl
from jax.experimental.pallas import tpu as pltpu
from jax.sharding import PartitionSpec as P

TOP_K = 2
GROUPS = 4
MESH = pl.DeviceIdType.MESH


NORM_EPS = 1e-06


def passed_along(value, axis, steps):
    count = lax.axis_size(axis)
    first, last = (max(0, -steps), min(count, count - steps))
    return lax.ppermute(value, axis, [(source, source + steps) for source in range(first, last)])


def general(
    b_gate,
    c_gate,
    h_in,
    docs,
    conv_taps,
    out_weight,
    residual_in,
    norm_gain,
    expert_pick,
    route_weight,
    w_gate,
    w_up,
    w_down,
):
    tok_rows, local_chans = h_in.shape
    width = residual_in.shape[1]
    full_dim = w_gate.shape[1]
    n_sp = lax.axis_size("sp")
    sp_index = lax.axis_index("sp")
    tp_index = lax.axis_index("tp")
    first_pos = sp_index * tok_rows
    product = (c_gate.astype(jnp.float32) * h_in.astype(jnp.float32)).astype(jnp.bfloat16)
    edge = passed_along(product[tok_rows - 2 :], "sp", 1)
    extended = jnp.concatenate([edge, product], axis=0).astype(jnp.float32)
    own_docs = lax.dynamic_slice_in_dim(docs, first_pos, tok_rows)
    padded_docs = jnp.concatenate([jnp.full((2,), -1, jnp.int32), docs], axis=0)
    near_docs = lax.dynamic_slice_in_dim(padded_docs, first_pos, tok_rows + 2)
    tap_weights = lax.dynamic_slice_in_dim(
        conv_taps, tp_index * local_chans, local_chans, 1
    ).astype(jnp.float32)
    conv_sum = tap_weights[0][None, :] * extended[2:]
    for step_back in (1, 2):
        same_doc = (near_docs[2 - step_back : 2 - step_back + tok_rows] == own_docs).astype(
            jnp.float32
        )[:, None]
        conv_sum = (
            conv_sum
            + tap_weights[step_back][None, :]
            * extended[2 - step_back : 2 - step_back + tok_rows]
            * same_doc
        )
    conv_out = (b_gate.astype(jnp.float32) * conv_sum).astype(jnp.bfloat16)
    projected = jnp.dot(
        lax.all_gather(conv_out, "tp", axis=1, tiled=True),
        out_weight,
        preferred_element_type=jnp.float32,
    )
    stream = (residual_in.astype(jnp.float32) + projected).astype(jnp.bfloat16)
    stream_f = stream.astype(jnp.float32)
    capacity = 5 * tok_rows // (2 * n_sp)
    assign_flat = expert_pick.reshape(-1)
    onehot = (assign_flat[:, None] == jnp.arange(n_sp, dtype=jnp.int32)[None, :]).astype(jnp.int32)
    slot_pos = jnp.sum((jnp.cumsum(onehot, axis=0) - onehot) * onehot, axis=1)
    kept_mask = slot_pos < capacity
    target = jnp.where(
        kept_mask, assign_flat * capacity + jnp.minimum(slot_pos, capacity - 1), n_sp * capacity
    )
    table = (
        jnp.full((n_sp * capacity + 1,), -1, jnp.int32)
        .at[target]
        .set(jnp.arange(assign_flat.shape[0], dtype=jnp.int32))[:-1]
    )
    filled = table >= 0
    source_rows = jnp.maximum(table, 0) // TOP_K
    gate_local = w_gate[0]
    up_local = w_up[0]
    slot_rows = n_sp * capacity
    squares = lax.psum(jnp.sum(stream_f * stream_f, axis=1), "tp")
    inverse = lax.rsqrt(squares / full_dim + NORM_EPS)[:, None]
    gain_cols = lax.dynamic_slice_in_dim(norm_gain, tp_index * width, width).astype(jnp.float32)
    normed = (stream_f * inverse * gain_cols[None, :]).astype(jnp.bfloat16)
    outgoing = jnp.where(filled[:, None], normed[source_rows], jnp.zeros((), normed.dtype)).reshape(
        n_sp, capacity, width
    )
    received = lax.all_to_all(outgoing, "sp", split_axis=0, concat_axis=0, tiled=True)
    shard_piece = lax.all_gather(received, "tp", axis=2, tiled=True)
    flat_piece = shard_piece.reshape(slot_rows, shard_piece.shape[2])
    gate_pre = jnp.dot(flat_piece, gate_local, preferred_element_type=jnp.float32)
    up_pre = jnp.dot(flat_piece, up_local, preferred_element_type=jnp.float32)
    hidden = (jax.nn.silu(gate_pre) * up_pre).astype(jnp.bfloat16)
    down_local = w_down[0]
    result = jnp.dot(
        lax.all_gather(hidden, "tp", axis=1, tiled=True),
        down_local,
        preferred_element_type=jnp.float32,
    ).astype(jnp.bfloat16)
    returned = lax.all_to_all(
        result.reshape(n_sp, capacity, width), "sp", split_axis=0, concat_axis=0, tiled=True
    ).reshape(n_sp * capacity, width)
    picked = jnp.where(
        kept_mask[:, None],
        returned[jnp.minimum(target, n_sp * capacity - 1)].astype(jnp.float32),
        0.0,
    )
    weighted = picked * route_weight.reshape(-1)[:, None]
    feed_out = jnp.sum(weighted.reshape(tok_rows, TOP_K, width), axis=1)
    return (stream_f + feed_out).astype(jnp.bfloat16)


def flipped(index, mask):
    bit = 1
    while bit <= mask:
        if mask & bit:
            index = index + bit * (1 - 2 * ((index // bit) % 2))
        bit *= 2
    return index


def fused_kernel(
    n_chips,
    capacity,
    docs_ref,
    pick_ref,
    rw_ref,
    taps_ref,
    gain_ref,
    b_hbm,
    c_hbm,
    h_hbm,
    resid_hbm,
    ow_hbm,
    wg_hbm,
    wu_hbm,
    wd_hbm,
    out_ref,
    bb,
    cc,
    hh,
    resid,
    ow,
    wg,
    wu,
    wd,
    ext,
    cv,
    side,
    gain,
    stream,
    acc,
    pt,
    ptt,
    rows_out,
    wts_out,
    rows,
    wts,
    normed,
    hid,
    e_own,
    e_send,
    e_recv,
    feed_out,
    back,
    local_sems,
    send_sems,
    recv_sems,
):
    tok_rows, chans = hh.shape
    width = resid.shape[1]
    full = gain.shape[1]
    hid_cols = wg.shape[1]
    f32, bf16 = jnp.float32, jnp.bfloat16
    sp = lax.axis_index("sp")
    tp = lax.axis_index("tp")
    chip = sp // 2
    core = sp % 2
    tp_x = (tp // 2) * 2 + (1 - tp % 2)
    tp_y = (1 - tp // 2) * 2 + tp % 2
    tp_d = (1 - tp // 2) * 2 + (1 - tp % 2)
    dev_x = (sp, tp_x)
    dev_y = (sp, tp_y)
    dev_s = (chip * 2 + (1 - core), tp)
    ks = list(range(n_chips))
    dev_z = [(flipped(chip, k) * 2 + core, tp) for k in ks]

    barrier = pltpu.get_barrier_semaphore()
    peers = [dev_x, dev_y, dev_s] + dev_z[1:]
    for dev in peers:
        pl.semaphore_signal(barrier, inc=1, device_id=dev, device_id_type=MESH)
    other = jnp.where(core == 0, sp - 1, sp + 1)
    has_other = jnp.where(core == 0, chip > 0, chip < n_chips - 1)

    @pl.when(has_other)
    def _():
        pl.semaphore_signal(barrier, inc=1, device_id=(other, tp), device_id_type=MESH)

    pairs = (
        (c_hbm, cc), (h_hbm, hh), (b_hbm, bb), (resid_hbm, resid),
        (ow_hbm, ow), (wg_hbm.at[0], wg), (wu_hbm.at[0], wu), (wd_hbm.at[0], wd),
    )
    loads = [pltpu.make_async_copy(s, d, local_sems.at[i]) for i, (s, d) in enumerate(pairs)]
    for cp in loads:
        cp.start()

    count = [0]
    sent = []

    def remote(s, d, dev):
        i = count[0]
        count[0] += 1
        return pltpu.make_async_remote_copy(
            src_ref=s, dst_ref=d, send_sem=send_sems.at[i], recv_sem=recv_sems.at[i],
            device_id=dev, device_id_type=MESH,
        )

    def go(s, d, dev):
        cp = remote(s, d, dev)
        cp.start()
        sent.append(cp)
        return cp

    def cols(index, size):
        return pl.ds(pl.multiple_of(index * size, 128), size)

    sub8 = lax.broadcasted_iota(jnp.int32, (8, tok_rows), 0)
    own = docs_ref[:, cols(sp, tok_rows)]
    prev = docs_ref[:, pl.ds(pl.multiple_of(jnp.maximum(sp * tok_rows - 128, 0), 128), 128)]
    prev = jnp.where(sp > 0, prev, -1)
    near = jnp.broadcast_to(jnp.concatenate([prev, own], axis=1), (8, tok_rows + 128))
    own = jnp.broadcast_to(own, (8, tok_rows))
    same = [(pltpu.roll(near, lag, 1)[:, 128:] == own).astype(f32) for lag in (1, 2)]
    first = pick_ref[0:1, :]
    even = jnp.bitwise_and(first, 1) == 0
    w_a, w_b = rw_ref[0:1, :], rw_ref[1:2, :]
    table = [
        lax.shift_right_logical(first, 1).astype(f32),
        jnp.where(even, w_a, w_b),
        jnp.where(even, w_b, w_a),
    ]
    block = jnp.where(sub8 == 0, same[0], jnp.where(sub8 == 1, same[1], 0.0))
    for i, row in enumerate(table):
        block = jnp.where(sub8 == 2 + i, jnp.broadcast_to(row, (8, tok_rows)), block)
    block = jnp.concatenate([block, jnp.zeros((120, tok_rows), f32)], axis=0)
    side[...] = jnp.transpose(block)

    loads[0].wait()
    loads[1].wait()
    product = (cc[...].astype(f32) * hh[...].astype(f32)).astype(bf16)
    ext[8:, :] = product.astype(f32)
    with jax.named_scope("barrier"):
        pl.semaphore_wait(barrier, len(peers) + has_other.astype(jnp.int32))

    edge = remote(ext.at[pl.ds(tok_rows, 8)], ext.at[pl.ds(0, 8)], (sp + 1, tp))

    @pl.when(sp < 2 * n_chips - 1)
    def _():
        edge.start()

    loads[2].wait()

    @pl.when(sp > 0)
    def _():
        with jax.named_scope("edge"):
            edge.wait_recv()

    @pl.when(sp == 0)
    def _():
        ext[0:8, :] = jnp.zeros((8, chans), f32)

    taps = taps_ref[:, cols(tp, chans)].astype(f32)
    conv = taps[0:1, :] * ext[8 : 8 + tok_rows, :]
    for lag in (1, 2):
        conv = conv + taps[lag : lag + 1, :] * ext[8 - lag : 8 - lag + tok_rows, :] * side[:, lag - 1 : lag]
    cv[:, cols(tp, chans)] = (bb[...].astype(f32) * conv).astype(bf16)

    def put(buf, at, dev):
        part = buf.at[:, at]
        return go(part, part, dev)

    def spread_one(buf, size, g):
        half = size // 2
        g["xh"] = put(buf, cols(tp * 2 + 1, half), dev_x)
        g["yl"] = put(buf, cols(tp * 2, half), dev_y)

    def spread_two(buf, size, g):
        half = size // 2
        g["xl"] = put(buf, cols(tp * 2, half), dev_x)
        g["yh"] = put(buf, cols(tp * 2 + 1, half), dev_y)

    def relay(buf, size, g):
        half = size // 2
        g["yl"].wait_recv()
        g["dl"] = put(buf, cols(tp_y * 2, half), dev_x)
        g["xh"].wait_recv()
        g["dh"] = put(buf, cols(tp_x * 2 + 1, half), dev_y)

    cg = {}
    spread_one(cv, chans, cg)
    spread_two(cv, chans, cg)

    def proj(index):
        rows_ = pl.ds(pl.multiple_of(index * chans, 128), chans)
        return jnp.dot(cv[:, cols(index, chans)], ow[rows_, :], preferred_element_type=f32)

    loads[3].wait()
    loads[4].wait()
    acc[...] = resid[...].astype(f32) + proj(tp)

    lane = lax.broadcasted_iota(jnp.int32, (tok_rows, 128), 1)
    lane_f = lane.astype(f32)
    group = side[:, 2:3]
    onehot = (group == lane_f).astype(f32)
    earlier = (
        lax.broadcasted_iota(jnp.int32, (tok_rows, tok_rows), 1)
        < lax.broadcasted_iota(jnp.int32, (tok_rows, tok_rows), 0)
    ).astype(f32).astype(bf16)
    before = jnp.dot(earlier, onehot.astype(bf16), preferred_element_type=f32)
    slot = jnp.sum(before * onehot, axis=1, keepdims=True)

    def choose(k):
        here = flipped(chip, k).astype(f32)
        hit = jnp.where((group == here) & (slot == lane_f) & (lane < capacity), 1.0, 0.0)
        pt[k] = hit.astype(bf16)
        ptt[k * capacity : (k + 1) * capacity, :] = jnp.transpose(hit)[:capacity].astype(bf16)
        w0 = jnp.sum(hit * side[:, 3:4], axis=0, keepdims=True)
        w1 = jnp.sum(hit * side[:, 4:5], axis=0, keepdims=True)
        s8 = lax.broadcasted_iota(jnp.int32, (8, 128), 0)
        w0, w1 = jnp.broadcast_to(w0, (8, 128)), jnp.broadcast_to(w1, (8, 128))
        wts_out[k] = jnp.where(s8 == 0, w0, jnp.where(s8 == 1, w1, 0.0))

    choose(0)
    choose(1)
    with jax.named_scope("crelay"):
        relay(cv, chans, cg)
    for k in ks[2:]:
        choose(k)
    wts[0] = wts_out[0]
    gains = gain_ref[...].astype(f32)
    for j in range(full // 128):
        gain[:, j * 128 : (j + 1) * 128] = gains[j : j + 1, :]
    with jax.named_scope("cx"):
        cg["xl"].wait_recv()
    acc[...] += proj(tp_x)
    with jax.named_scope("cy"):
        cg["yh"].wait_recv()
    acc[...] += proj(tp_y)
    with jax.named_scope("cd"):
        cg["dl"].wait_recv()
        cg["dh"].wait_recv()
    stream[...] = (acc[...] + proj(tp_d)).astype(bf16)

    mine = cols(tp, width)
    rg, hg = [{} for _ in ks], [{} for _ in ks]
    sis = [[] for _ in ks]
    z_rows, z_wts, e_sends, z_back = [[None] * n_chips for _ in range(4)]

    def share(k, index, size):
        at = cols(index, size)
        sis[k].append(go(rows.at[k, 0, :, at], rows.at[k, 1, :, at], dev_s))

    def select(k):
        at = slice(k * capacity, (k + 1) * capacity)
        return jnp.dot(ptt[at, :], stream[...], preferred_element_type=f32).astype(bf16)

    def rows_send(k):
        if k == 0:
            rows[0, 0, :, mine] = select(0)
        else:
            z_rows[k].wait_recv()
        spread_one(rows.at[k, 0], width, rg[k])
        spread_two(rows.at[k, 0], width, rg[k])
        share(k, tp, width)

    def z_send(k):
        rows_out[k] = select(k)
        z_rows[k] = go(rows_out.at[k], rows.at[k, 0, :, mine], dev_z[k])
        z_wts[k] = go(wts_out.at[k], wts.at[k], dev_z[k])

    def rows_relay(k):
        relay(rows.at[k, 0], width, rg[k])

    def rows_near(k):
        rg[k]["xl"].wait_recv()
        share(k, tp_x, width)
        rg[k]["yh"].wait_recv()
        share(k, tp_y, width)

    def rows_far(k):
        rg[k]["dl"].wait_recv()
        share(k, tp_d * 2, width // 2)
        rg[k]["dh"].wait_recv()
        share(k, tp_d * 2 + 1, width // 2)

    def norm(k, p):
        if p == 1:
            for cp in sis[k]:
                cp.wait_recv()

        def body(r, carry):
            at = pl.ds(pl.multiple_of(r * 16, 16), 16)
            x = rows[k, p, at, :].astype(f32)
            ms = jnp.sum(x * x, axis=1, keepdims=True) / full
            inv = lax.rsqrt(ms + NORM_EPS)
            y = (x * inv * gain[...]).astype(bf16)
            normed[pl.ds(pl.multiple_of(p * capacity + r * 16, 16), 16), :] = y
            return carry

        lax.fori_loop(0, capacity // 16, body, 0)

    def up(k):
        if k == 0:
            loads[5].wait()
            loads[6].wait()

        def tile(n, carry):
            at = pl.ds(pl.multiple_of(n * 256, 256), 256)
            x = normed[...]
            g = jnp.dot(x, wg[:, at], preferred_element_type=f32)
            u = jnp.dot(x, wu[:, at], preferred_element_type=f32)
            h = (g / (1.0 + jnp.exp(-g)) * u).astype(bf16)
            hid[k, :, pl.ds(pl.multiple_of(tp * hid_cols + n * 256, 256), 256)] = h
            return carry

        lax.fori_loop(0, hid_cols // 256, tile, 0)

    def hid_one(k):
        spread_one(hid.at[k], hid_cols, hg[k])

    def hid_two(k):
        spread_two(hid.at[k], hid_cols, hg[k])

    def hid_relay(k):
        relay(hid.at[k], hid_cols, hg[k])

    waited = []

    def down(k):
        for name in ("xl", "yh", "dl", "dh"):
            hg[k][name].wait_recv()
        if not waited:
            loads[7].wait()
            waited.append(k)

        def tile(n, carry):
            at = pl.ds(pl.multiple_of(n * 256, 256), 256)
            e = jnp.dot(hid[k], wd[:, at], preferred_element_type=f32).astype(bf16)
            e_own[k, :, at] = e[:capacity]
            e_send[k, :, at] = e[capacity:]
            return carry

        lax.fori_loop(0, width // 256, tile, 0)
        e_sends[k] = go(e_send.at[k], e_recv.at[k], dev_s)

    def column(row):
        l128 = lax.broadcasted_iota(jnp.int32, (capacity, 128), 1)
        s128 = lax.broadcasted_iota(jnp.int32, (capacity, 128), 0)
        return jnp.sum(jnp.where(l128 == s128, row, 0.0), axis=1, keepdims=True)

    def combine(k):
        if k > 0:
            z_wts[k].wait_recv()
        w = wts[k]
        w_even, w_odd = column(w[0:1, :]), column(w[1:2, :])
        pick = core.astype(f32)
        w_mine = w_even * (1.0 - pick) + w_odd * pick
        w_other = w_odd * (1.0 - pick) + w_even * pick
        e_sends[k].wait_recv()
        f = (e_own[k].astype(f32) * w_mine + e_recv[k].astype(f32) * w_other).astype(bf16)
        if k == 0:
            back[0, 0:capacity, :] = f
        else:
            feed_out[k] = f
            z_back[k] = go(feed_out.at[k], back.at[k, pl.ds(0, capacity), :], dev_z[k])

    def gather(k):
        if k > 0:
            z_back[k].wait_recv()
        got = jnp.dot(pt[k], back[k], preferred_element_type=f32)
        if k == 0:
            out_ref[...] = (acc[...] + got).astype(bf16)
        else:
            acc[...] += got

    def clear():
        acc[...] = stream[...].astype(f32)
        for k in ks:
            back[k, capacity:, :] = jnp.zeros((128 - capacity, width), bf16)

    def near_far(k):
        rows_near(k)
        rows_far(k)

    plan = [
        (rows_send, 0), (z_send, 1), (clear,), (rows_relay, 0), (z_send, 2), (rows_near, 0), (rows_send, 1),
        (rows_far, 0), (z_send, 3), (norm, 0, 0), (rows_relay, 1), (norm, 0, 1), (up, 0), (rows_send, 2),
        (near_far, 1), (norm, 1, 0), (rows_relay, 2), (norm, 1, 1), (up, 1), (rows_send, 3), (near_far, 2),
        (norm, 2, 0), (rows_relay, 3), (norm, 2, 1), (up, 2), (hid_one, 2), (hid_two, 2), (hid_one, 0),
        (near_far, 3), (norm, 3, 0), (hid_relay, 2), (norm, 3, 1), (up, 3), (hid_one, 3), (hid_two, 3),
        (hid_one, 1), (down, 2), (hid_relay, 3), (hid_two, 1), (combine, 2), (hid_relay, 1), (hid_two, 0),
        (hid_relay, 0), (down, 3), (combine, 3), (down, 1), (combine, 1), (gather, 2), (down, 0), (combine, 0),
        (gather, 3), (gather, 1), (gather, 0),
    ]

    for step, *args in plan:
        name = step.__name__ + "".join("_" + str(a) for a in args)
        with jax.named_scope(name):
            step(*args)

    with jax.named_scope("drain"):
        for cp in sent:
            cp.wait_send()

        @pl.when(sp < 2 * n_chips - 1)
        def _():
            edge.wait_send()


def fused(
    b_gate,
    c_gate,
    h_in,
    docs,
    conv_taps,
    out_weight,
    residual_in,
    norm_gain,
    expert_pick,
    route_weight,
    w_gate,
    w_up,
    w_down,
):
    tok_rows, chans = h_in.shape
    width = residual_in.shape[1]
    full = w_gate.shape[1]
    hid_full = w_down.shape[1]
    n_sp = lax.axis_size("sp")
    n_chips = n_sp // 2
    capacity = 5 * tok_rows // (2 * n_sp)
    n_copies = 7 + 18 * n_chips + 3 * (n_chips - 1)
    vmem = pl.BlockSpec(memory_space=pltpu.VMEM)
    hbm = pl.BlockSpec(memory_space=pltpu.HBM)
    bf16, f32 = jnp.bfloat16, jnp.float32
    return pl.pallas_call(
        functools.partial(fused_kernel, n_chips, capacity),
        out_shape=pltpu.VMEM((tok_rows, width), bf16),
        in_specs=[vmem] * 5 + [hbm] * 8,
        out_specs=vmem,
        scratch_shapes=[
            pltpu.VMEM(b_gate.shape, bf16),
            pltpu.VMEM(c_gate.shape, bf16),
            pltpu.VMEM(h_in.shape, bf16),
            pltpu.VMEM(residual_in.shape, bf16),
            pltpu.VMEM(out_weight.shape, bf16),
            pltpu.VMEM(w_gate.shape[1:], bf16),
            pltpu.VMEM(w_up.shape[1:], bf16),
            pltpu.VMEM(w_down.shape[1:], bf16),
            pltpu.VMEM((tok_rows + 8, chans), f32),
            pltpu.VMEM((tok_rows, out_weight.shape[0]), bf16),
            pltpu.VMEM((tok_rows, 128), f32),
            pltpu.VMEM((1, full), f32),
            pltpu.VMEM((tok_rows, width), bf16),
            pltpu.VMEM((tok_rows, width), f32),
            pltpu.VMEM((n_chips, tok_rows, 128), bf16),
            pltpu.VMEM((n_chips * capacity, tok_rows), bf16),
            pltpu.VMEM((n_chips, capacity, width), bf16),
            pltpu.VMEM((n_chips, 8, 128), f32),
            pltpu.VMEM((n_chips, 2, capacity, full), bf16),
            pltpu.VMEM((n_chips, 8, 128), f32),
            pltpu.VMEM((2 * capacity, full), bf16),
            pltpu.VMEM((n_chips, 2 * capacity, hid_full), bf16),
            pltpu.VMEM((n_chips, capacity, width), bf16),
            pltpu.VMEM((n_chips, capacity, width), bf16),
            pltpu.VMEM((n_chips, capacity, width), bf16),
            pltpu.VMEM((n_chips, capacity, width), bf16),
            pltpu.VMEM((n_chips, 128, width), bf16),
            pltpu.SemaphoreType.DMA((8,)),
            pltpu.SemaphoreType.DMA((n_copies,)),
            pltpu.SemaphoreType.DMA((n_copies,)),
        ],
        compiler_params=pltpu.CompilerParams(
            collective_id=0, has_side_effects=True, vmem_limit_bytes=66519040
        ),
    )(
        docs.reshape(1, -1),
        expert_pick.T,
        route_weight.T,
        conv_taps,
        norm_gain.reshape(-1, 128),
        b_gate,
        c_gate,
        h_in,
        residual_in,
        out_weight,
        w_gate,
        w_up,
        w_down,
    )


def pairs_fit(mesh):
    n_sp, n_tp = mesh.shape["sp"], mesh.shape["tp"]
    return n_sp == GROUPS * TOP_K and TOP_K == 2 and n_tp == 4


def solution(mesh):
    return jax.shard_map(
        fused if pairs_fit(mesh) else general,
        mesh=mesh,
        in_specs=(
            P("sp", "tp"),
            P("sp", "tp"),
            P("sp", "tp"),
            P(),
            P(),
            P(None, "tp"),
            P("sp", "tp"),
            P(),
            P("sp", None),
            P("sp", None),
            P("sp", None, "tp"),
            P("sp", None, "tp"),
            P("sp", None, "tp"),
        ),
        out_specs=P("sp", "tp"),
        check_vma=False,
    )
```

time: 87.9 us -> 75.2 us (0.86)
  Pallas kernels: 80 us -> 74.2 us
  other arithmetic: 3.6 us -> 0 us
  local copies, waits for them, and re-layouts: 3.46 us -> 0.8 us
    pallas_call x1, Pallas kernels: 80 us -> 74.2 us  [fused(): pl.pallas_call(functools.partial(fused_kernel, n_chips, capacity), out_sh...]
    select_n x2 -> x0, other arithmetic: 1.53 us -> none  [the longest x1 0.77 us: fused(): jnp.where(even, route_weight[:, 1], route_weight[:, 0])]
    broadcast_in_dim x1 -> x0, other arithmetic: 1.3 us -> none  [fused(): gain = norm_gain.astype(jnp.float32)[None, :]]
    unnamed x1, local copies, waits for them, and re-layouts: 1.87 us -> 0.8 us
where the time goes in v1:
time: 75.2 us; the launch traced here: 75 us
  Pallas kernels  74.2 us (99%)
  local copies, waits for them, and re-layouts  0.8 us (1%)
    pallas_call x1, Pallas kernels, fused(): pl.pallas_call(functools.partial(fused_kernel, n_chips, capacity), out_sh...  74.2 us

profile of v1, /device:TPU:0, one launch (start us, length us, event | category | flops | bytes accessed | tf_op | source)
XLA Modules:
  0.0 75.0 jit_solution(17128673302541957539)
XLA Ops:
  0.0 74.2 %shard_map.127 = bf16[256,1024]{1,0:T(8,128)(2,1)S(1)} custom-call(s32[1,2048]{1,0:T(1,128)} %bitcast.4, s32[2,256]{1,0:T(2,128)} %bitcast.6, f32[2,256]{1,0:T(2,128)} %bitcast.7, bf16[3,1024]{1,0:T(4,128)(2,1)} %taps_ref.1, bf16[32,128]{1,0:T(8,128)(2,1)} %bitcast.5, bf16[256,256]{1,0:T(8,128)(2,1)} %b_hbm.1, bf16[256,256]{1,0:T(8,128)(2,1)} %c_hbm.1, ...), custom_call_target="tpu_custom_call" | custom-call | tf_op jit(solution)/shard_map/pallas_call | solution.py:557
  74.2 0.8 %copy.15 = bf16[256,1024]{1,0:T(8,128)(2,1)} copy(bf16[256,1024]{1,0:T(8,128)(2,1)S(1)} %shard_map.127) | data formatting | bytes 1048576

commit v2 on v1

--- a/solution.py
+++ b/solution.py
@@ -174,6 +174,7 @@
     e_recv,
     feed_out,
     back,
+    up_sems,
     local_sems,
     send_sems,
     recv_sems,
@@ -192,20 +193,25 @@
     tp_d = (1 - tp // 2) * 2 + (1 - tp % 2)
     dev_x = (sp, tp_x)
     dev_y = (sp, tp_y)
+    dev_d = (sp, tp_d)
     dev_s = (chip * 2 + (1 - core), tp)
     ks = list(range(n_chips))
     dev_z = [(flipped(chip, k) * 2 + core, tp) for k in ks]
 
     barrier = pltpu.get_barrier_semaphore()
-    peers = [dev_x, dev_y, dev_s] + dev_z[1:]
-    for dev in peers:
-        pl.semaphore_signal(barrier, inc=1, device_id=dev, device_id_type=MESH)
-    other = jnp.where(core == 0, sp - 1, sp + 1)
-    has_other = jnp.where(core == 0, chip > 0, chip < n_chips - 1)
-
-    @pl.when(has_other)
-    def _():
-        pl.semaphore_signal(barrier, inc=1, device_id=(other, tp), device_id_type=MESH)
+    plane = [dev_x, dev_y, dev_d, dev_s]
+    above = [flipped(chip, k) > chip for k in ks]
+    edge_down = (core == 0) & (chip > 0)
+    edge_up = (core == 1) & (chip < n_chips - 1)
+
+    def signal(sem, dev):
+        pl.semaphore_signal(sem, inc=1, device_id=dev, device_id_type=MESH)
+
+    for dev in plane:
+        signal(barrier, dev)
+    for k in ks[1:]:
+        pl.when(above[k])(functools.partial(signal, barrier, dev_z[k]))
+    pl.when(edge_up)(functools.partial(signal, barrier, (sp + 1, tp)))
 
     pairs = (
         (c_hbm, cc), (h_hbm, hh), (b_hbm, bb), (resid_hbm, resid),
@@ -215,22 +221,42 @@
     for cp in loads:
         cp.start()
 
-    count = [0]
+    count = [2, 0]
+    room = [rows.size * 2, hid.size * 2]
     sent = []
 
-    def remote(s, d, dev):
-        i = count[0]
-        count[0] += 1
-        return pltpu.make_async_remote_copy(
-            src_ref=s, dst_ref=d, send_sem=send_sems.at[i], recv_sem=recv_sems.at[i],
+    def recv_sem():
+        count[1] += 1
+        return recv_sems.at[count[1] - 1]
+
+    def remote(s, d, dev, recv=None, own_send=False):
+        size = s.size * jnp.dtype(s.dtype).itemsize
+        fits = [i for i in (0, 1) if room[i] >= size and size % (capacity * width) == 0]
+        if fits:
+            i = fits[0]
+            room[i] -= size
+        else:
+            i = count[0]
+            count[0] += 1
+        cp = pltpu.make_async_remote_copy(
+            src_ref=s, dst_ref=d, send_sem=send_sems.at[i],
+            recv_sem=recv_sem() if recv is None else recv,
             device_id=dev, device_id_type=MESH,
         )
-
-    def go(s, d, dev):
-        cp = remote(s, d, dev)
+        if not fits and not own_send:
+            sent.append(cp)
+        return cp
+
+    def go(s, d, dev, recv=None, own_send=False):
+        cp = remote(s, d, dev, recv, own_send)
         cp.start()
-        sent.append(cp)
         return cp
+
+    def await_bytes(ref, recv):
+        pltpu.make_async_remote_copy(
+            src_ref=ref, dst_ref=ref, send_sem=send_sems.at[0], recv_sem=recv,
+            device_id=dev_x, device_id_type=MESH,
+        ).wait_recv()
 
     def cols(index, size):
         return pl.ds(pl.multiple_of(index * size, 128), size)
@@ -261,63 +287,76 @@
     product = (cc[...].astype(f32) * hh[...].astype(f32)).astype(bf16)
     ext[8:, :] = product.astype(f32)
     with jax.named_scope("barrier"):
-        pl.semaphore_wait(barrier, len(peers) + has_other.astype(jnp.int32))
-
-    edge = remote(ext.at[pl.ds(tok_rows, 8)], ext.at[pl.ds(0, 8)], (sp + 1, tp))
-
-    @pl.when(sp < 2 * n_chips - 1)
-    def _():
-        edge.start()
-
+        pl.semaphore_wait(barrier, len(plane) + chip + edge_down.astype(jnp.int32))
+    for k in ks[1:]:
+        pl.when(flipped(chip, k) < chip)(functools.partial(signal, up_sems.at[k], dev_z[k]))
+    pl.when(edge_down)(functools.partial(signal, up_sems.at[0], (sp - 1, tp)))
+
+    edge = remote(ext.at[pl.ds(tok_rows, 8)], ext.at[pl.ds(0, 8)], (sp + 1, tp), None, True)
+    pl.when(core == 0)(edge.start)
     loads[2].wait()
-
-    @pl.when(sp > 0)
-    def _():
-        with jax.named_scope("edge"):
-            edge.wait_recv()
-
-    @pl.when(sp == 0)
-    def _():
-        ext[0:8, :] = jnp.zeros((8, chans), f32)
-
     taps = taps_ref[:, cols(tp, chans)].astype(f32)
-    conv = taps[0:1, :] * ext[8 : 8 + tok_rows, :]
-    for lag in (1, 2):
-        conv = conv + taps[lag : lag + 1, :] * ext[8 - lag : 8 - lag + tok_rows, :] * side[:, lag - 1 : lag]
-    cv[:, cols(tp, chans)] = (bb[...].astype(f32) * conv).astype(bf16)
-
-    def put(buf, at, dev):
+
+    def conv(lo, hi):
+        total = taps[0:1, :] * ext[8 + lo : 8 + hi, :]
+        for lag in (1, 2):
+            part = ext[8 + lo - lag : 8 + hi - lag, :]
+            total = total + taps[lag : lag + 1, :] * part * side[lo:hi, lag - 1 : lag]
+        cv[lo:hi, cols(tp, chans)] = (bb[lo:hi, :].astype(f32) * total).astype(bf16)
+
+    head = 16
+    conv(head, tok_rows)
+
+    def put(buf, at, dev, recv=None, own_send=False):
         part = buf.at[:, at]
-        return go(part, part, dev)
-
-    def spread_one(buf, size, g):
-        half = size // 2
-        g["xh"] = put(buf, cols(tp * 2 + 1, half), dev_x)
-        g["yl"] = put(buf, cols(tp * 2, half), dev_y)
-
-    def spread_two(buf, size, g):
-        half = size // 2
-        g["xl"] = put(buf, cols(tp * 2, half), dev_x)
-        g["yh"] = put(buf, cols(tp * 2 + 1, half), dev_y)
+        return go(part, part, dev, recv, own_send)
+
+    def send_yl(buf, size, g):
+        g["yl"] = put(buf, cols(tp * 2, size // 2), dev_y)
+
+    def send_xh(buf, size, g):
+        g["xh"] = put(buf, cols(tp * 2 + 1, size // 2), dev_x)
+
+    def send_xl(buf, size, g):
+        put(buf, cols(tp * 2, size // 2), dev_x, g["late"])
+
+    def send_yh(buf, size, g):
+        put(buf, cols(tp * 2 + 1, size // 2), dev_y, g["late"])
+
+    def spread(buf, size, g):
+        g["late"] = recv_sem()
+        for send in (send_yl, send_xh, send_xl, send_yh):
+            send(buf, size, g)
+
+    def relay_x(buf, size, g):
+        g["yl"].wait_recv()
+        if "far" not in g:
+            g["far"] = recv_sem()
+        put(buf, cols(tp_y * 2, size // 2), dev_x, g["far"])
+
+    def relay_y(buf, size, g):
+        g["xh"].wait_recv()
+        if "far" not in g:
+            g["far"] = recv_sem()
+        put(buf, cols(tp_x * 2 + 1, size // 2), dev_y, g["far"])
 
     def relay(buf, size, g):
-        half = size // 2
-        g["yl"].wait_recv()
-        g["dl"] = put(buf, cols(tp_y * 2, half), dev_x)
-        g["xh"].wait_recv()
-        g["dh"] = put(buf, cols(tp_x * 2 + 1, half), dev_y)
+        relay_x(buf, size, g)
+        relay_y(buf, size, g)
 
     cg = {}
-    spread_one(cv, chans, cg)
-    spread_two(cv, chans, cg)
+    body = cv.at[pl.ds(head, tok_rows - head)]
+    spread(body, chans, cg)
 
     def proj(index):
         rows_ = pl.ds(pl.multiple_of(index * chans, 128), chans)
         return jnp.dot(cv[:, cols(index, chans)], ow[rows_, :], preferred_element_type=f32)
 
-    loads[3].wait()
-    loads[4].wait()
-    acc[...] = resid[...].astype(f32) + proj(tp)
+    @pl.when(edge_up)
+    def _():
+        pl.semaphore_wait(up_sems.at[0], 1)
+        edge.start()
+
 
     lane = lax.broadcasted_iota(jnp.int32, (tok_rows, 128), 1)
     lane_f = lane.astype(f32)
@@ -342,34 +381,49 @@
         wts_out[k] = jnp.where(s8 == 0, w0, jnp.where(s8 == 1, w1, 0.0))
 
     choose(0)
-    choose(1)
+
+    @pl.when(sp > 0)
+    def _():
+        with jax.named_scope("edge"):
+            edge.wait_recv()
+
+    @pl.when(sp == 0)
+    def _():
+        ext[0:8, :] = jnp.zeros((8, chans), f32)
+
+    conv(0, head)
+    top, top_sem = cv.at[pl.ds(0, head), cols(tp, chans)], recv_sem()
+    for dev in (dev_x, dev_y, dev_d):
+        go(top, top, dev, top_sem)
+    loads[3].wait()
+    loads[4].wait()
+    acc[...] = resid[...].astype(f32) + proj(tp)
     with jax.named_scope("crelay"):
-        relay(cv, chans, cg)
-    for k in ks[2:]:
+        relay(body, chans, cg)
+    for k in ks[1:]:
         choose(k)
     wts[0] = wts_out[0]
     gains = gain_ref[...].astype(f32)
     for j in range(full // 128):
         gain[:, j * 128 : (j + 1) * 128] = gains[j : j + 1, :]
+    with jax.named_scope("top"):
+        await_bytes(cv.at[pl.ds(0, head), pl.ds(0, 3 * chans)], top_sem)
     with jax.named_scope("cx"):
-        cg["xl"].wait_recv()
+        await_bytes(body.at[:, pl.ds(0, chans)], cg["late"])
     acc[...] += proj(tp_x)
-    with jax.named_scope("cy"):
-        cg["yh"].wait_recv()
     acc[...] += proj(tp_y)
     with jax.named_scope("cd"):
-        cg["dl"].wait_recv()
-        cg["dh"].wait_recv()
+        await_bytes(body.at[:, pl.ds(0, chans)], cg["far"])
     stream[...] = (acc[...] + proj(tp_d)).astype(bf16)
 
     mine = cols(tp, width)
     rg, hg = [{} for _ in ks], [{} for _ in ks]
-    sis = [[] for _ in ks]
-    z_rows, z_wts, e_sends, z_back = [[None] * n_chips for _ in range(4)]
+    sis = [recv_sem() for _ in ks]
+    z_rows, z_wts = [None] * n_chips, [None] * n_chips
 
     def share(k, index, size):
         at = cols(index, size)
-        sis[k].append(go(rows.at[k, 0, :, at], rows.at[k, 1, :, at], dev_s))
+        go(rows.at[k, 0, :, at], rows.at[k, 1, :, at], dev_s, sis[k])
 
     def select(k):
         at = slice(k * capacity, (k + 1) * capacity)
@@ -380,34 +434,51 @@
             rows[0, 0, :, mine] = select(0)
         else:
             z_rows[k].wait_recv()
-        spread_one(rows.at[k, 0], width, rg[k])
-        spread_two(rows.at[k, 0], width, rg[k])
+        spread(rows.at[k, 0], width, rg[k])
         share(k, tp, width)
 
-    def z_send(k):
+    def z_pick(k):
         rows_out[k] = select(k)
-        z_rows[k] = go(rows_out.at[k], rows.at[k, 0, :, mine], dev_z[k])
-        z_wts[k] = go(wts_out.at[k], wts.at[k], dev_z[k])
-
-    def rows_relay(k):
-        relay(rows.at[k, 0], width, rg[k])
+        z_rows[k] = remote(rows_out.at[k], rows.at[k, 0, :, mine], dev_z[k])
+        z_wts[k] = remote(wts_out.at[k], wts.at[k], dev_z[k])
+
+    def z_go(k, when=None):
+        def start():
+            @pl.when(above[k])
+            def _():
+                pl.semaphore_wait(up_sems.at[k], 1)
+
+            z_rows[k].start()
+            z_wts[k].start()
+
+        start() if when is None else pl.when(when)(start)
+
+    inner = jnp.abs(flipped(chip, ks[-1]) - chip) == 1
+
+    def z_inner():
+        z_go(ks[-1], inner)
+
+    def z_outer():
+        z_go(ks[-1], jnp.logical_not(inner))
+
+    def rows_rx(k):
+        relay_x(rows.at[k, 0], width, rg[k])
+
+    def rows_ry(k):
+        relay_y(rows.at[k, 0], width, rg[k])
 
     def rows_near(k):
-        rg[k]["xl"].wait_recv()
+        await_bytes(rows.at[k, 0, :, pl.ds(0, width)], rg[k]["late"])
         share(k, tp_x, width)
-        rg[k]["yh"].wait_recv()
         share(k, tp_y, width)
 
     def rows_far(k):
-        rg[k]["dl"].wait_recv()
-        share(k, tp_d * 2, width // 2)
-        rg[k]["dh"].wait_recv()
-        share(k, tp_d * 2 + 1, width // 2)
+        await_bytes(rows.at[k, 0, :, pl.ds(0, width)], rg[k]["far"])
+        share(k, tp_d, width)
 
     def norm(k, p):
         if p == 1:
-            for cp in sis[k]:
-                cp.wait_recv()
+            await_bytes(rows.at[k, 1], sis[k])
 
         def body(r, carry):
             at = pl.ds(pl.multiple_of(r * 16, 16), 16)
@@ -420,98 +491,110 @@
 
         lax.fori_loop(0, capacity // 16, body, 0)
 
-    def up(k):
-        if k == 0:
+    def up(k, n):
+        if k == 0 and n == 0:
             loads[5].wait()
             loads[6].wait()
+        half = hid_cols // 2
+        at = slice(n * half, (n + 1) * half)
+        x = normed[...]
+        g = jnp.dot(x, wg[:, at], preferred_element_type=f32)
+        u = jnp.dot(x, wu[:, at], preferred_element_type=f32)
+        hid[k, :, cols(tp * 2 + n, half)] = (g / (1.0 + jnp.exp(-g)) * u).astype(bf16)
+
+    senders = {"yl": send_yl, "xh": send_xh, "xl": send_xl, "yh": send_yh}
+
+    def hs(k, name):
+        if not hg[k]:
+            hg[k]["late"] = hg[k]["far"] = recv_sem()
+        senders[name](hid.at[k], hid_cols, hg[k])
+
+    def hid_rx(k):
+        relay_x(hid.at[k], hid_cols, hg[k])
+
+    def hid_ry(k):
+        relay_y(hid.at[k], hid_cols, hg[k])
+
+    begun = []
+    e_sends, z_back = {}, {}
+    half_width = width // 2
+    halves = [slice(h * half_width, (h + 1) * half_width) for h in (0, 1)]
+
+    def down(k, h):
+        if k not in begun:
+            await_bytes(hid.at[k, :, pl.ds(0, 2 * hid_cols)], hg[k]["late"])
+        if not begun:
+            loads[7].wait()
+        begun.append(k)
 
         def tile(n, carry):
-            at = pl.ds(pl.multiple_of(n * 256, 256), 256)
-            x = normed[...]
-            g = jnp.dot(x, wg[:, at], preferred_element_type=f32)
-            u = jnp.dot(x, wu[:, at], preferred_element_type=f32)
-            h = (g / (1.0 + jnp.exp(-g)) * u).astype(bf16)
-            hid[k, :, pl.ds(pl.multiple_of(tp * hid_cols + n * 256, 256), 256)] = h
-            return carry
-
-        lax.fori_loop(0, hid_cols // 256, tile, 0)
-
-    def hid_one(k):
-        spread_one(hid.at[k], hid_cols, hg[k])
-
-    def hid_two(k):
-        spread_two(hid.at[k], hid_cols, hg[k])
-
-    def hid_relay(k):
-        relay(hid.at[k], hid_cols, hg[k])
-
-    waited = []
-
-    def down(k):
-        for name in ("xl", "yh", "dl", "dh"):
-            hg[k][name].wait_recv()
-        if not waited:
-            loads[7].wait()
-            waited.append(k)
-
-        def tile(n, carry):
-            at = pl.ds(pl.multiple_of(n * 256, 256), 256)
+            at = pl.ds(pl.multiple_of(h * half_width + n * 256, 256), 256)
             e = jnp.dot(hid[k], wd[:, at], preferred_element_type=f32).astype(bf16)
             e_own[k, :, at] = e[:capacity]
             e_send[k, :, at] = e[capacity:]
             return carry
 
-        lax.fori_loop(0, width // 256, tile, 0)
-        e_sends[k] = go(e_send.at[k], e_recv.at[k], dev_s)
+        lax.fori_loop(0, half_width // 256, tile, 0)
+        at = halves[h]
+        e_sends[k, h] = go(e_send.at[k, :, at], e_recv.at[k, :, at], dev_s)
 
     def column(row):
         l128 = lax.broadcasted_iota(jnp.int32, (capacity, 128), 1)
         s128 = lax.broadcasted_iota(jnp.int32, (capacity, 128), 0)
         return jnp.sum(jnp.where(l128 == s128, row, 0.0), axis=1, keepdims=True)
 
-    def combine(k):
+    weights = {}
+
+    def combine(k, h):
+        if k not in weights:
+            if k > 0:
+                z_wts[k].wait_recv()
+            w = wts[k]
+            w_even, w_odd = column(w[0:1, :]), column(w[1:2, :])
+            pick = core.astype(f32)
+            weights[k] = (
+                w_even * (1.0 - pick) + w_odd * pick, w_odd * (1.0 - pick) + w_even * pick
+            )
+        w_mine, w_other = weights[k]
+        at = halves[h]
+        e_sends[k, h].wait_recv()
+        f = (e_own[k, :, at].astype(f32) * w_mine + e_recv[k, :, at].astype(f32) * w_other).astype(bf16)
+        if k == 0:
+            back[0, 0:capacity, at] = f
+        else:
+            feed_out[k, :, at] = f
+            z_back[k, h] = go(feed_out.at[k, :, at], back.at[k, pl.ds(0, capacity), at], dev_z[k])
+
+    def gather(k, h):
         if k > 0:
-            z_wts[k].wait_recv()
-        w = wts[k]
-        w_even, w_odd = column(w[0:1, :]), column(w[1:2, :])
-        pick = core.astype(f32)
-        w_mine = w_even * (1.0 - pick) + w_odd * pick
-        w_other = w_odd * (1.0 - pick) + w_even * pick
-        e_sends[k].wait_recv()
-        f = (e_own[k].astype(f32) * w_mine + e_recv[k].astype(f32) * w_other).astype(bf16)
+            z_back[k, h].wait_recv()
+        at = halves[h]
+        got = jnp.dot(pt[k], back[k, :, at], preferred_element_type=f32)
         if k == 0:
-            back[0, 0:capacity, :] = f
+            out_ref[:, at] = (acc[:, at] + got).astype(bf16)
         else:
-            feed_out[k] = f
-            z_back[k] = go(feed_out.at[k], back.at[k, pl.ds(0, capacity), :], dev_z[k])
-
-    def gather(k):
-        if k > 0:
-            z_back[k].wait_recv()
-        got = jnp.dot(pt[k], back[k], preferred_element_type=f32)
-        if k == 0:
-            out_ref[...] = (acc[...] + got).astype(bf16)
-        else:
-            acc[...] += got
+            acc[:, at] += got
 
     def clear():
         acc[...] = stream[...].astype(f32)
         for k in ks:
             back[k, capacity:, :] = jnp.zeros((128 - capacity, width), bf16)
 
-    def near_far(k):
-        rows_near(k)
-        rows_far(k)
-
     plan = [
-        (rows_send, 0), (z_send, 1), (clear,), (rows_relay, 0), (z_send, 2), (rows_near, 0), (rows_send, 1),
-        (rows_far, 0), (z_send, 3), (norm, 0, 0), (rows_relay, 1), (norm, 0, 1), (up, 0), (rows_send, 2),
-        (near_far, 1), (norm, 1, 0), (rows_relay, 2), (norm, 1, 1), (up, 1), (rows_send, 3), (near_far, 2),
-        (norm, 2, 0), (rows_relay, 3), (norm, 2, 1), (up, 2), (hid_one, 2), (hid_two, 2), (hid_one, 0),
-        (near_far, 3), (norm, 3, 0), (hid_relay, 2), (norm, 3, 1), (up, 3), (hid_one, 3), (hid_two, 3),
-        (hid_one, 1), (down, 2), (hid_relay, 3), (hid_two, 1), (combine, 2), (hid_relay, 1), (hid_two, 0),
-        (hid_relay, 0), (down, 3), (combine, 3), (down, 1), (combine, 1), (gather, 2), (down, 0), (combine, 0),
-        (gather, 3), (gather, 1), (gather, 0),
+        (rows_send, 0), (z_pick, 1), (z_go, 1), (z_pick, 2), (z_go, 2), (z_pick, 3), (rows_rx, 0),
+        (rows_ry, 0), (rows_send, 1), (z_outer,), (rows_near, 0), (rows_ry, 1), (rows_far, 0), (rows_rx, 1),
+        (norm, 0, 0), (z_inner,), (rows_send, 2), (norm, 0, 1), (up, 0, 0), (rows_near, 1), (up, 0, 1),
+        (rows_rx, 2), (rows_far, 1), (rows_ry, 2), (rows_send, 3), (hs, 0, "xh"), (norm, 1, 0),
+        (norm, 1, 1), (up, 1, 0), (rows_near, 2), (rows_far, 2), (up, 1, 1), (norm, 2, 0), (rows_ry, 3),
+        (norm, 2, 1), (rows_rx, 3), (up, 2, 0), (hs, 2, "yl"), (up, 2, 1), (hs, 1, "yl"), (rows_near, 3),
+        (hs, 2, "xh"), (hs, 2, "xl"), (rows_far, 3), (hs, 2, "yh"), (norm, 3, 0), (hid_rx, 2), (norm, 3, 1),
+        (hid_ry, 2), (up, 3, 0), (hs, 3, "xl"), (hs, 3, "yl"), (up, 3, 1), (hs, 3, "xh"), (hs, 1, "xh"),
+        (clear,), (hs, 3, "yh"), (hs, 1, "yh"), (down, 2, 1), (down, 2, 0), (hid_rx, 3), (combine, 2, 1),
+        (hid_rx, 1), (hid_ry, 3), (hid_ry, 1), (hs, 0, "yl"), (hid_ry, 0), (combine, 2, 0), (hs, 1, "xl"),
+        (down, 3, 0), (down, 3, 1), (hs, 0, "yh"), (combine, 3, 0), (hs, 0, "xl"), (down, 1, 0),
+        (down, 1, 1), (hid_rx, 0), (combine, 1, 0), (gather, 2, 0), (combine, 1, 1), (combine, 3, 1),
+        (down, 0, 1), (down, 0, 0), (gather, 1, 1), (gather, 2, 1), (gather, 3, 0), (combine, 0, 0),
+        (gather, 1, 0), (combine, 0, 1), (gather, 0, 0), (gather, 3, 1), (gather, 0, 1),
     ]
 
     for step, *args in plan:
@@ -520,12 +603,16 @@
             step(*args)
 
     with jax.named_scope("drain"):
+        for i, ref in enumerate((rows, hid)):
+            pltpu.make_async_remote_copy(
+                src_ref=ref, dst_ref=ref, send_sem=send_sems.at[i], recv_sem=recv_sems.at[0],
+                device_id=dev_x, device_id_type=MESH,
+            ).wait_send()
         for cp in sent:
             cp.wait_send()
-
-        @pl.when(sp < 2 * n_chips - 1)
-        def _():
-            edge.wait_send()
+        pl.when(sp < 2 * n_chips - 1)(edge.wait_send)
+        if any(room) or count[0] != send_sems.shape[0] or count[1] != recv_sems.shape[0]:
+            raise ValueError(f"semaphores {room} {count}")
 
 
 def fused(
@@ -550,7 +637,6 @@
     n_sp = lax.axis_size("sp")
     n_chips = n_sp // 2
     capacity = 5 * tok_rows // (2 * n_sp)
-    n_copies = 7 + 18 * n_chips + 3 * (n_chips - 1)
     vmem = pl.BlockSpec(memory_space=pltpu.VMEM)
     hbm = pl.BlockSpec(memory_space=pltpu.HBM)
     bf16, f32 = jnp.bfloat16, jnp.float32
@@ -587,9 +673,10 @@
             pltpu.VMEM((n_chips, capacity, width), bf16),
             pltpu.VMEM((n_chips, capacity, width), bf16),
             pltpu.VMEM((n_chips, 128, width), bf16),
+            pltpu.SemaphoreType.REGULAR((n_chips,)),
             pltpu.SemaphoreType.DMA((8,)),
-            pltpu.SemaphoreType.DMA((n_copies,)),
-            pltpu.SemaphoreType.DMA((n_copies,)),
+            pltpu.SemaphoreType.DMA((19,)),
+            pltpu.SemaphoreType.DMA((58,)),
         ],
         compiler_params=pltpu.CompilerParams(
             collective_id=0, has_side_effects=True, vmem_limit_bytes=66519040

time: 75.2 us -> 67.5 us (0.90)
  Pallas kernels: 74.2 us -> 66.5 us
    pallas_call x1, Pallas kernels: 74.2 us -> 66.5 us  [fused(): pl.pallas_call(functools.partial(fused_kernel, n_chips, capacity), out_sh...]
where the time goes in v2:
time: 67.5 us; the launch traced here: 67.3 us
  Pallas kernels  66.5 us (99%)
  local copies, waits for them, and re-layouts  0.8 us (1%)
    pallas_call x1, Pallas kernels, fused(): pl.pallas_call(functools.partial(fused_kernel, n_chips, capacity), out_sh...  66.5 us

profile of v2, /device:TPU:0, one launch (start us, length us, event | category | flops | bytes accessed | tf_op | source)
XLA Modules:
  0.0 67.3 jit_solution(1556025827643319209)
XLA Ops:
  0.0 66.5 %shard_map.127 = bf16[256,1024]{1,0:T(8,128)(2,1)S(1)} custom-call(s32[1,2048]{1,0:T(1,128)} %bitcast.4, s32[2,256]{1,0:T(2,128)} %bitcast.6, f32[2,256]{1,0:T(2,128)} %bitcast.7, bf16[3,1024]{1,0:T(4,128)(2,1)} %taps_ref.1, bf16[32,128]{1,0:T(8,128)(2,1)} %bitcast.5, bf16[256,256]{1,0:T(8,128)(2,1)} %b_hbm.1, bf16[256,256]{1,0:T(8,128)(2,1)} %c_hbm.1, ...), custom_call_target="tpu_custom_call" | custom-call | tf_op jit(solution)/shard_map/pallas_call | solution.py:643
  66.5 0.8 %copy.15 = bf16[256,1024]{1,0:T(8,128)(2,1)} copy(bf16[256,1024]{1,0:T(8,128)(2,1)S(1)} %shard_map.127) | data formatting | bytes 1048576

commit v3 on v2

--- a/solution.py
+++ b/solution.py
@@ -133,11 +133,11 @@
 def fused_kernel(
     n_chips,
     capacity,
-    docs_ref,
-    pick_ref,
-    rw_ref,
-    taps_ref,
-    gain_ref,
+    docs_hbm,
+    pick_hbm,
+    rw_hbm,
+    taps_hbm,
+    gain_hbm,
     b_hbm,
     c_hbm,
     h_hbm,
@@ -147,6 +147,11 @@
     wu_hbm,
     wd_hbm,
     out_ref,
+    docs_ref,
+    pick_ref,
+    rw_ref,
+    taps_ref,
+    gain_ref,
     bb,
     cc,
     hh,
@@ -174,6 +179,7 @@
     e_recv,
     feed_out,
     back,
+    partial,
     up_sems,
     local_sems,
     send_sems,
@@ -184,6 +190,7 @@
     full = gain.shape[1]
     hid_cols = wg.shape[1]
     f32, bf16 = jnp.float32, jnp.bfloat16
+    head = 16
     sp = lax.axis_index("sp")
     tp = lax.axis_index("tp")
     chip = sp // 2
@@ -199,7 +206,7 @@
     dev_z = [(flipped(chip, k) * 2 + core, tp) for k in ks]
 
     barrier = pltpu.get_barrier_semaphore()
-    plane = [dev_x, dev_y, dev_d, dev_s]
+    plane = [dev_x, dev_y, dev_s]
     above = [flipped(chip, k) > chip for k in ks]
     edge_down = (core == 0) & (chip > 0)
     edge_up = (core == 1) & (chip < n_chips - 1)
@@ -212,18 +219,28 @@
     for k in ks[1:]:
         pl.when(above[k])(functools.partial(signal, barrier, dev_z[k]))
     pl.when(edge_up)(functools.partial(signal, barrier, (sp + 1, tp)))
+    pl.when(edge_down)(functools.partial(signal, barrier, (sp - 1, tp)))
 
     pairs = (
-        (c_hbm, cc), (h_hbm, hh), (b_hbm, bb), (resid_hbm, resid),
+        (c_hbm, cc), (h_hbm, hh), (docs_hbm, docs_ref), (pick_hbm, pick_ref), (rw_hbm, rw_ref),
+        (taps_hbm, taps_ref), (gain_hbm, gain_ref), (b_hbm, bb), (resid_hbm, resid),
         (ow_hbm, ow), (wg_hbm.at[0], wg), (wu_hbm.at[0], wu), (wd_hbm.at[0], wd),
     )
     loads = [pltpu.make_async_copy(s, d, local_sems.at[i]) for i, (s, d) in enumerate(pairs)]
     for cp in loads:
         cp.start()
 
-    count = [2, 0]
-    room = [rows.size * 2, hid.size * 2]
-    sent = []
+    unit = capacity * width
+    groups = [
+        (rows, unit),
+        (hid, unit),
+        (rows.at[0, 0, :, pl.ds(0, 2 * width)], unit),
+        (cv.at[pl.ds(head, tok_rows - head), pl.ds(0, 3 * chans)], (tok_rows - head) * chans),
+        (cv.at[pl.ds(0, head), pl.ds(0, 3 * chans)], head * chans * 2),
+        (wts_out.at[pl.ds(1, n_chips - 1)], 8 * 128 * 4),
+    ]
+    room = [ref.size * jnp.dtype(ref.dtype).itemsize for ref, _ in groups]
+    count = [len(groups), 0]
 
     def recv_sem():
         count[1] += 1
@@ -231,20 +248,17 @@
 
     def remote(s, d, dev, recv=None, own_send=False):
         size = s.size * jnp.dtype(s.dtype).itemsize
-        fits = [i for i in (0, 1) if room[i] >= size and size % (capacity * width) == 0]
-        if fits:
-            i = fits[0]
-            room[i] -= size
-        else:
+        if own_send:
             i = count[0]
             count[0] += 1
+        else:
+            i = [j for j, (_, step) in enumerate(groups) if room[j] >= size and size % step == 0][0]
+            room[i] -= size
         cp = pltpu.make_async_remote_copy(
             src_ref=s, dst_ref=d, send_sem=send_sems.at[i],
             recv_sem=recv_sem() if recv is None else recv,
             device_id=dev, device_id_type=MESH,
         )
-        if not fits and not own_send:
-            sent.append(cp)
         return cp
 
     def go(s, d, dev, recv=None, own_send=False):
@@ -261,6 +275,8 @@
     def cols(index, size):
         return pl.ds(pl.multiple_of(index * size, 128), size)
 
+    for i in (2, 3, 4):
+        loads[i].wait()
     sub8 = lax.broadcasted_iota(jnp.int32, (8, tok_rows), 0)
     own = docs_ref[:, cols(sp, tok_rows)]
     prev = docs_ref[:, pl.ds(pl.multiple_of(jnp.maximum(sp * tok_rows - 128, 0), 128), 128)]
@@ -287,14 +303,15 @@
     product = (cc[...].astype(f32) * hh[...].astype(f32)).astype(bf16)
     ext[8:, :] = product.astype(f32)
     with jax.named_scope("barrier"):
-        pl.semaphore_wait(barrier, len(plane) + chip + edge_down.astype(jnp.int32))
+        pl.semaphore_wait(barrier, len(plane) + chip + (edge_down | edge_up).astype(jnp.int32))
     for k in ks[1:]:
         pl.when(flipped(chip, k) < chip)(functools.partial(signal, up_sems.at[k], dev_z[k]))
-    pl.when(edge_down)(functools.partial(signal, up_sems.at[0], (sp - 1, tp)))
+    signal(up_sems.at[0], dev_x)
 
     edge = remote(ext.at[pl.ds(tok_rows, 8)], ext.at[pl.ds(0, 8)], (sp + 1, tp), None, True)
-    pl.when(core == 0)(edge.start)
-    loads[2].wait()
+    pl.when(sp < 2 * n_chips - 1)(edge.start)
+    loads[7].wait()
+    loads[5].wait()
     taps = taps_ref[:, cols(tp, chans)].astype(f32)
 
     def conv(lo, hi):
@@ -304,7 +321,6 @@
             total = total + taps[lag : lag + 1, :] * part * side[lo:hi, lag - 1 : lag]
         cv[lo:hi, cols(tp, chans)] = (bb[lo:hi, :].astype(f32) * total).astype(bf16)
 
-    head = 16
     conv(head, tok_rows)
 
     def put(buf, at, dev, recv=None, own_send=False):
@@ -351,11 +367,6 @@
     def proj(index):
         rows_ = pl.ds(pl.multiple_of(index * chans, 128), chans)
         return jnp.dot(cv[:, cols(index, chans)], ow[rows_, :], preferred_element_type=f32)
-
-    @pl.when(edge_up)
-    def _():
-        pl.semaphore_wait(up_sems.at[0], 1)
-        edge.start()
 
 
     lane = lax.broadcasted_iota(jnp.int32, (tok_rows, 128), 1)
@@ -393,16 +404,19 @@
 
     conv(0, head)
     top, top_sem = cv.at[pl.ds(0, head), cols(tp, chans)], recv_sem()
-    for dev in (dev_x, dev_y, dev_d):
-        go(top, top, dev, top_sem)
-    loads[3].wait()
-    loads[4].wait()
+    go(top, top, dev_x, top_sem)
+    go(top, top, dev_y, top_sem)
+    pl.semaphore_wait(up_sems.at[0], 1)
+    go(top, top, dev_d, top_sem)
+    loads[8].wait()
+    loads[9].wait()
     acc[...] = resid[...].astype(f32) + proj(tp)
     with jax.named_scope("crelay"):
         relay(body, chans, cg)
     for k in ks[1:]:
         choose(k)
     wts[0] = wts_out[0]
+    loads[6].wait()
     gains = gain_ref[...].astype(f32)
     for j in range(full // 128):
         gain[:, j * 128 : (j + 1) * 128] = gains[j : j + 1, :]
@@ -419,7 +433,9 @@
     mine = cols(tp, width)
     rg, hg = [{} for _ in ks], [{} for _ in ks]
     sis = [recv_sem() for _ in ks]
-    z_rows, z_wts = [None] * n_chips, [None] * n_chips
+    z_rows, z_wts = {}, {}
+    half_width = width // 2
+    halves = [slice(h * half_width, (h + 1) * half_width) for h in (0, 1)]
 
     def share(k, index, size):
         at = cols(index, size)
@@ -429,17 +445,25 @@
         at = slice(k * capacity, (k + 1) * capacity)
         return jnp.dot(ptt[at, :], stream[...], preferred_element_type=f32).astype(bf16)
 
-    def rows_send(k):
-        if k == 0:
+    def rows_send(k, part):
+        h = 1 if part == "hi" else 0
+        if k > 0:
+            z_rows[k, h].wait_recv()
+        elif h == 1:
             rows[0, 0, :, mine] = select(0)
-        else:
-            z_rows[k].wait_recv()
-        spread(rows.at[k, 0], width, rg[k])
-        share(k, tp, width)
+        buf = rows.at[k, 0]
+        if "late" not in rg[k]:
+            rg[k]["late"] = recv_sem()
+        for send in (send_xh, send_yh) if h else (send_yl, send_xl):
+            send(buf, width, rg[k])
+        share(k, tp * 2 + h, half_width)
 
     def z_pick(k):
         rows_out[k] = select(k)
-        z_rows[k] = remote(rows_out.at[k], rows.at[k, 0, :, mine], dev_z[k])
+        for h in (1, 0):
+            at = cols(tp * 2 + h, width // 2)
+            src = rows_out.at[k, :, halves[h]]
+            z_rows[k, h] = remote(src, rows.at[k, 0, :, at], dev_z[k])
         z_wts[k] = remote(wts_out.at[k], wts.at[k], dev_z[k])
 
     def z_go(k, when=None):
@@ -448,7 +472,8 @@
             def _():
                 pl.semaphore_wait(up_sems.at[k], 1)
 
-            z_rows[k].start()
+            z_rows[k, 1].start()
+            z_rows[k, 0].start()
             z_wts[k].start()
 
         start() if when is None else pl.when(when)(start)
@@ -480,21 +505,20 @@
         if p == 1:
             await_bytes(rows.at[k, 1], sis[k])
 
-        def body(r, carry):
-            at = pl.ds(pl.multiple_of(r * 16, 16), 16)
-            x = rows[k, p, at, :].astype(f32)
+        for r in range(capacity // 16):
+            x = rows[k, p, r * 16 : (r + 1) * 16, :].astype(f32)
             ms = jnp.sum(x * x, axis=1, keepdims=True) / full
             inv = lax.rsqrt(ms + NORM_EPS)
-            y = (x * inv * gain[...]).astype(bf16)
-            normed[pl.ds(pl.multiple_of(p * capacity + r * 16, 16), 16), :] = y
-            return carry
-
-        lax.fori_loop(0, capacity // 16, body, 0)
+            first = p * capacity + r * 16
+            normed[first : first + 16, :] = (x * inv * gain[...]).astype(bf16)
+
+    started = []
 
     def up(k, n):
-        if k == 0 and n == 0:
-            loads[5].wait()
-            loads[6].wait()
+        if not started:
+            loads[10].wait()
+            loads[11].wait()
+        started.append(k)
         half = hid_cols // 2
         at = slice(n * half, (n + 1) * half)
         x = normed[...]
@@ -506,7 +530,8 @@
 
     def hs(k, name):
         if not hg[k]:
-            hg[k]["late"] = hg[k]["far"] = recv_sem()
+            hg[k]["late"] = recv_sem()
+            hg[k]["far"] = recv_sem() if k == 0 else hg[k]["late"]
         senders[name](hid.at[k], hid_cols, hg[k])
 
     def hid_rx(k):
@@ -517,19 +542,44 @@
 
     begun = []
     e_sends, z_back = {}, {}
-    half_width = width // 2
-    halves = [slice(h * half_width, (h + 1) * half_width) for h in (0, 1)]
+
+    def fetch_down():
+        if not begun:
+            loads[12].wait()
+        begun.append(-1)
+
+    def dot_down(k, index, at):
+        rows_ = pl.ds(pl.multiple_of(index * hid_cols, 128), hid_cols)
+        part = hid[k, :, cols(index, hid_cols)]
+        return jnp.dot(part, wd[rows_, at], preferred_element_type=f32)
+
+    def dpre(k):
+        await_bytes(hid.at[k, :, pl.ds(0, hid_cols)], hg[k]["late"])
+        fetch_down()
+
+        def tile(n, carry):
+            at = pl.ds(pl.multiple_of(n * 256, 256), 256)
+            partial[:, at] = dot_down(k, tp, at) + dot_down(k, tp_x, at) + dot_down(k, tp_y, at)
+            return carry
+
+        lax.fori_loop(0, width // 256, tile, 0)
 
     def down(k, h):
         if k not in begun:
-            await_bytes(hid.at[k, :, pl.ds(0, 2 * hid_cols)], hg[k]["late"])
-        if not begun:
-            loads[7].wait()
+            if k == 0:
+                await_bytes(hid.at[k, :, pl.ds(0, hid_cols)], hg[k]["far"])
+            else:
+                await_bytes(hid.at[k, :, pl.ds(0, 2 * hid_cols)], hg[k]["late"])
+        fetch_down()
         begun.append(k)
 
         def tile(n, carry):
             at = pl.ds(pl.multiple_of(h * half_width + n * 256, 256), 256)
-            e = jnp.dot(hid[k], wd[:, at], preferred_element_type=f32).astype(bf16)
+            if k == 0:
+                e = partial[:, at] + dot_down(k, tp_d, at)
+            else:
+                e = jnp.dot(hid[k], wd[:, at], preferred_element_type=f32)
+            e = e.astype(bf16)
             e_own[k, :, at] = e[:capacity]
             e_send[k, :, at] = e[capacity:]
             return carry
@@ -581,20 +631,22 @@
             back[k, capacity:, :] = jnp.zeros((128 - capacity, width), bf16)
 
     plan = [
-        (rows_send, 0), (z_pick, 1), (z_go, 1), (z_pick, 2), (z_go, 2), (z_pick, 3), (rows_rx, 0),
-        (rows_ry, 0), (rows_send, 1), (z_outer,), (rows_near, 0), (rows_ry, 1), (rows_far, 0), (rows_rx, 1),
-        (norm, 0, 0), (z_inner,), (rows_send, 2), (norm, 0, 1), (up, 0, 0), (rows_near, 1), (up, 0, 1),
-        (rows_rx, 2), (rows_far, 1), (rows_ry, 2), (rows_send, 3), (hs, 0, "xh"), (norm, 1, 0),
-        (norm, 1, 1), (up, 1, 0), (rows_near, 2), (rows_far, 2), (up, 1, 1), (norm, 2, 0), (rows_ry, 3),
-        (norm, 2, 1), (rows_rx, 3), (up, 2, 0), (hs, 2, "yl"), (up, 2, 1), (hs, 1, "yl"), (rows_near, 3),
-        (hs, 2, "xh"), (hs, 2, "xl"), (rows_far, 3), (hs, 2, "yh"), (norm, 3, 0), (hid_rx, 2), (norm, 3, 1),
-        (hid_ry, 2), (up, 3, 0), (hs, 3, "xl"), (hs, 3, "yl"), (up, 3, 1), (hs, 3, "xh"), (hs, 1, "xh"),
-        (clear,), (hs, 3, "yh"), (hs, 1, "yh"), (down, 2, 1), (down, 2, 0), (hid_rx, 3), (combine, 2, 1),
-        (hid_rx, 1), (hid_ry, 3), (hid_ry, 1), (hs, 0, "yl"), (hid_ry, 0), (combine, 2, 0), (hs, 1, "xl"),
-        (down, 3, 0), (down, 3, 1), (hs, 0, "yh"), (combine, 3, 0), (hs, 0, "xl"), (down, 1, 0),
-        (down, 1, 1), (hid_rx, 0), (combine, 1, 0), (gather, 2, 0), (combine, 1, 1), (combine, 3, 1),
-        (down, 0, 1), (down, 0, 0), (gather, 1, 1), (gather, 2, 1), (gather, 3, 0), (combine, 0, 0),
-        (gather, 1, 0), (combine, 0, 1), (gather, 0, 0), (gather, 3, 1), (gather, 0, 1),
+        (z_pick, 1), (z_go, 1), (rows_send, 0, "hi"), (z_pick, 3), (z_inner,), (z_pick, 2),
+        (rows_send, 0, "lo"), (rows_send, 1, "hi"), (rows_send, 1, "lo"), (z_outer,), (z_go, 2), (clear,),
+        (rows_send, 3, "hi"), (rows_send, 3, "lo"), (rows_ry, 1), (rows_rx, 1), (rows_rx, 0), (rows_ry, 3),
+        (rows_near, 1), (rows_rx, 3), (rows_send, 2, "hi"), (rows_far, 1), (rows_send, 2, "lo"),
+        (norm, 1, 0), (norm, 1, 1), (up, 1, 0), (rows_ry, 0), (rows_near, 0), (rows_near, 3), (rows_far, 3),
+        (up, 1, 1), (hs, 1, "yh"), (norm, 3, 0), (hs, 1, "xl"), (norm, 3, 1), (up, 3, 0), (rows_rx, 2),
+        (rows_ry, 2), (hs, 3, "yl"), (rows_far, 0), (hs, 1, "yl"), (up, 3, 1), (hs, 3, "xh"), (hs, 3, "xl"),
+        (norm, 0, 0), (rows_near, 2), (norm, 0, 1), (hs, 3, "yh"), (up, 0, 0), (up, 0, 1), (rows_far, 2),
+        (hs, 1, "xh"), (hid_rx, 3), (hid_ry, 3), (norm, 2, 0), (norm, 2, 1), (up, 2, 0), (hs, 2, "yl"),
+        (up, 2, 1), (hs, 2, "xh"), (hid_rx, 1), (hid_ry, 1), (hs, 2, "xl"), (down, 3, 0), (hs, 2, "yh"),
+        (hid_ry, 2), (hid_rx, 2), (combine, 3, 0), (hs, 0, "xh"), (hs, 0, "yl"), (down, 3, 1), (down, 1, 0),
+        (down, 1, 1), (hs, 0, "xl"), (hs, 0, "yh"), (combine, 3, 1), (combine, 1, 0), (down, 2, 1),
+        (combine, 2, 1), (hid_rx, 0), (combine, 1, 1), (hid_ry, 0), (down, 2, 0), (dpre, 0),
+        (combine, 2, 0), (down, 0, 1), (gather, 3, 1), (down, 0, 0), (gather, 1, 0), (gather, 3, 0),
+        (combine, 0, 1), (gather, 2, 1), (combine, 0, 0), (gather, 1, 1), (gather, 0, 1), (gather, 2, 0),
+        (gather, 0, 0),
     ]
 
     for step, *args in plan:
@@ -603,13 +655,11 @@
             step(*args)
 
     with jax.named_scope("drain"):
-        for i, ref in enumerate((rows, hid)):
+        for i, (ref, _) in enumerate(groups):
             pltpu.make_async_remote_copy(
                 src_ref=ref, dst_ref=ref, send_sem=send_sems.at[i], recv_sem=recv_sems.at[0],
                 device_id=dev_x, device_id_type=MESH,
             ).wait_send()
-        for cp in sent:
-            cp.wait_send()
         pl.when(sp < 2 * n_chips - 1)(edge.wait_send)
         if any(room) or count[0] != send_sems.shape[0] or count[1] != recv_sems.shape[0]:
             raise ValueError(f"semaphores {room} {count}")
@@ -643,9 +693,14 @@
     return pl.pallas_call(
         functools.partial(fused_kernel, n_chips, capacity),
         out_shape=pltpu.VMEM((tok_rows, width), bf16),
-        in_specs=[vmem] * 5 + [hbm] * 8,
+        in_specs=[hbm] * 13,
         out_specs=vmem,
         scratch_shapes=[
+            pltpu.VMEM((1, docs.shape[0]), jnp.int32),
+            pltpu.VMEM((2, tok_rows), jnp.int32),
+            pltpu.VMEM((2, tok_rows), f32),
+            pltpu.VMEM(conv_taps.shape, bf16),
+            pltpu.VMEM((full // 128, 128), bf16),
             pltpu.VMEM(b_gate.shape, bf16),
             pltpu.VMEM(c_gate.shape, bf16),
             pltpu.VMEM(h_in.shape, bf16),
@@ -673,10 +728,11 @@
             pltpu.VMEM((n_chips, capacity, width), bf16),
             pltpu.VMEM((n_chips, capacity, width), bf16),
             pltpu.VMEM((n_chips, 128, width), bf16),
+            pltpu.VMEM((2 * capacity, width), f32),
             pltpu.SemaphoreType.REGULAR((n_chips,)),
-            pltpu.SemaphoreType.DMA((8,)),
-            pltpu.SemaphoreType.DMA((19,)),
-            pltpu.SemaphoreType.DMA((58,)),
+            pltpu.SemaphoreType.DMA((13,)),
+            pltpu.SemaphoreType.DMA((7,)),
+            pltpu.SemaphoreType.DMA((62,)),
         ],
         compiler_params=pltpu.CompilerParams(
             collective_id=0, has_side_effects=True, vmem_limit_bytes=66519040

time: 67.5 us -> 65.9 us (0.976)
  Pallas kernels: 66.5 us -> 65 us
    pallas_call x1, Pallas kernels: 66.5 us -> 65 us  [fused(): pl.pallas_call(functools.partial(fused_kernel, n_chips, capacity), out_sh...]
where the time goes in v3:
time: 65.9 us; the launch traced here: 65.8 us
  Pallas kernels  65 us (99%)
  local copies, waits for them, and re-layouts  0.8 us (1%)
    pallas_call x1, Pallas kernels, fused(): pl.pallas_call(functools.partial(fused_kernel, n_chips, capacity), out_sh...  65 us

profile of v3, /device:TPU:0, one launch (start us, length us, event | category | flops | bytes accessed | tf_op | source)
XLA Modules:
  0.0 65.8 jit_solution(321685283033727141)
XLA Ops:
  0.0 65.0 %shard_map.127 = bf16[256,1024]{1,0:T(8,128)(2,1)S(1)} custom-call(s32[1,2048]{1,0:T(1,128)} %bitcast.4, s32[2,256]{1,0:T(2,128)} %bitcast.6, f32[2,256]{1,0:T(2,128)} %bitcast.7, bf16[3,1024]{1,0:T(4,128)(2,1)} %taps_hbm.1, bf16[32,128]{1,0:T(8,128)(2,1)} %bitcast.5, bf16[256,256]{1,0:T(8,128)(2,1)} %b_hbm.1, bf16[256,256]{1,0:T(8,128)(2,1)} %c_hbm.1, ...), custom_call_target="tpu_custom_call" | custom-call | tf_op jit(solution)/shard_map/pallas_call | solution.py:693
  65.0 0.8 %copy.15 = bf16[256,1024]{1,0:T(8,128)(2,1)} copy(bf16[256,1024]{1,0:T(8,128)(2,1)S(1)} %shard_map.127) | data formatting | bytes 1048576
